TPU v7x, 32 devices: a whole 2x2x4 slice. The times are simulated.
32 devices in a mesh: fs: 8 (over z, y), tp: 4 (over x, core).
Axes of the slice: x: 2, y: 2, z: 4, core: 2. Of those that a mesh axis runs over, the one named last changes fastest.
Arguments:
- hidden_in: bfloat16 [512, 4096], P(None, 'tp'), may hold values from -6 to 6
- up_act: bfloat16 [512, 12288], P('tp', 'fs'), may hold values from -6 to 6
- up_val: bfloat16 [512, 12288], P('tp', 'fs'), may hold values from -6 to 6
- cotangent: bfloat16 [512, 4096], P('tp'), may hold values from -6 to 6
- w_act: bfloat16 [4096, 12288], P('tp', 'fs'), may hold values from -0.09375 to 0.09375
- w_val: bfloat16 [4096, 12288], P('tp', 'fs'), may hold values from -0.09375 to 0.09375
- w_down: bfloat16 [12288, 4096], P('fs', 'tp'), may hold values from -0.0546875 to 0.0546875
- conv_act: bfloat16 [3, 12288], P(None, 'fs'), may hold values from -3 to 3
- conv_val: bfloat16 [3, 12288], P(None, 'fs'), may hold values from -3 to 3
- bias_act: bfloat16 [12288], P('fs'), may hold values from -3 to 3
- bias_val: bfloat16 [12288], P('fs'), may hold values from -3 to 3
Outputs:
- grad_input: bfloat16 [512, 4096], P(('tp', 'fs'))
- grad_w_act: float32 [4096, 12288], P('tp', 'fs')
- grad_w_val: float32 [4096, 12288], P('tp', 'fs')
- grad_w_down: float32 [12288, 4096], P('fs', 'tp')
- grad_conv_act: float32 [3, 12288], P(None, 'fs')
- grad_conv_val: float32 [3, 12288], P(None, 'fs')
- grad_bias_act: float32 [12288], P('fs')
- grad_bias_val: float32 [12288], P('fs')
- rows_act: float32 [4096], P('tp')
- rows_val: float32 [4096], P('tp')
- rows_down: float32 [12288], P('fs')
- conv_rows: float32 [2, 3], replicated
All inputs are finite; a program needn't handle non-finite values.
Results may differ from a plain program's by a relative error of at most 0.0057.
Values may be sent and summed in bfloat16 or wider, within the bound.
A program may use at most 128 MiB of HBM per device.

v0:
```python
import jax
import jax.numpy as jnp
from jax import lax
from jax.experimental import pallas as pl
from jax.experimental.pallas import tpu as pltpu
from jax.sharding import PartitionSpec as P

MESH = pl.DeviceIdType.MESH
F32 = jnp.float32
BF16 = jnp.bfloat16
CHUNK = 256
HALO = 16
TAIL = 8
ROOT_TWO_OVER_PI = 0.7978845608028654
CUBIC = 0.044715


def remote(copy_at, source, target, send, receive, where):
    return pltpu.make_async_remote_copy(
        src_ref=source,
        dst_ref=target,
        send_sem=send.at[copy_at],
        recv_sem=receive.at[copy_at],
        device_id=where,
        device_id_type=MESH,
    )


def greet(everyone):
    barrier = pltpu.get_barrier_semaphore()
    for where in everyone:
        pl.semaphore_signal(barrier, inc=1, device_id=where, device_id_type=MESH)
    pl.semaphore_wait(barrier, len(everyone))


def gradient_kernel(
    cot, down, up_a, up_v, taps_a, taps_v, bias_a, bias_v, weights_a, weights_v,
    columns, all_a, all_v, all_m, sums, terms,
    own, to_sib, to_sib_far, to_far, from_sib, from_sib_far, from_far,
    before_a, before_v, grad_a, grad_v, after_a, after_v, own_sums, got_sums,
    gated, factor, held_a, held_v,
    send, receive, loaded,
):
    me = lax.axis_index("tp")
    count = lax.axis_size("tp")
    chip, core = me // 2, me % 2
    sib = chip * 2 + (1 - core)
    far = (1 - chip) * 2 + core
    diag = (1 - chip) * 2 + (1 - core)
    right, left = lax.rem(me + 1, count), lax.rem(me + count - 1, count)
    length, width = up_a.shape
    depth = down.shape[1]
    tap_count = taps_a.shape[0]
    reach = tap_count - 1

    def to(index):
        return {"tp": index}

    def rows(ref, index):
        return ref.at[pl.ds(pl.multiple_of(index * length, length), length), :]

    def cols(index):
        return pl.ds(pl.multiple_of(index * depth, depth), depth)

    loads = [
        pltpu.make_async_copy(weights_a, held_a, loaded.at[0]),
        pltpu.make_async_copy(weights_v, held_v, loaded.at[1]),
    ]
    for load in loads:
        load.start()
    greet([to(sib), to(far), to(diag)])
    cot_copies = [
        remote(slot, cot.at[:, cols(peer)], rows(columns, me), send, receive, to(peer))
        for slot, peer in ((0, sib), (1, far), (2, diag))
    ]
    last = pl.ds(length - HALO, HALO)
    halo_copies = [
        remote(3, up_a.at[last, :], before_a, send, receive, to(right)),
        remote(4, up_v.at[last, :], before_v, send, receive, to(right)),
    ]
    for copy in (cot_copies[1], cot_copies[2], cot_copies[0], *halo_copies):
        copy.start()
    rows(columns, me)[...] = cot[:, cols(me)]

    def partial(index, finish):
        block = rows(columns, index)[...]

        def step(at, carry):
            lanes = pl.ds(pl.multiple_of(at * CHUNK, CHUNK), CHUNK)
            finish(lanes, contract_last(block, down[lanes, :]))
            return carry

        lax.fori_loop(0, width // CHUNK, step, 0)

    def keep(target):
        def finish(lanes, value):
            target[:, lanes] = value.astype(target.dtype)

        return finish

    def add_far(lanes, value):
        to_far[:, lanes] = (value + from_sib_far[:, lanes].astype(F32)).astype(BF16)

    has_before = (me > 0).astype(F32)
    has_after = (me < count - 1).astype(F32)
    out_m, out_a, out_v = rows(all_m, me), rows(all_a, me), rows(all_v, me)

    def shifted(before, up, lanes):
        ext = jnp.concatenate(
            [before[:, lanes].astype(F32) * has_before, up[:, lanes].astype(F32)], 0
        )
        return [ext[HALO - reach + k : HALO - reach + k + length] for k in range(tap_count)]

    def forward(at, carry):
        lanes = pl.ds(pl.multiple_of(at * CHUNK, CHUNK), CHUNK)
        taken_a, taken_v = shifted(before_a, up_a, lanes), shifted(before_v, up_v, lanes)
        pre_a = jnp.broadcast_to(bias_a[:, lanes].astype(F32), (length, CHUNK))
        pre_v = jnp.broadcast_to(bias_v[:, lanes].astype(F32), (length, CHUNK))
        for k in range(tap_count):
            pre_a = pre_a + taps_a[k : k + 1, lanes].astype(F32) * taken_a[k]
            pre_v = pre_v + taps_v[k : k + 1, lanes].astype(F32) * taken_v[k]
        square = pre_a * pre_a
        bent = jnp.tanh(ROOT_TWO_OVER_PI * pre_a * (1.0 + CUBIC * square))
        half = 0.5 * (1.0 + bent)
        gelu = pre_a * half
        slope = half + 0.5 * pre_a * (1.0 - bent * bent) * (
            ROOT_TWO_OVER_PI * (1.0 + 3.0 * CUBIC * square)
        )
        out_m[:, lanes] = (gelu * pre_v).astype(BF16)
        gated[:, lanes] = gelu
        factor[:, lanes] = pre_v * slope
        return carry

    def spread(slot, ref):
        pair = [
            remote(10 + slot, rows(ref, me), rows(ref, me), send, receive, to(far)),
            remote(13 + slot, rows(ref, me), rows(ref, me), send, receive, to(sib)),
        ]
        for copy in pair:
            copy.start()
        return pair

    partial(me, keep(own))
    for copy in halo_copies:
        copy.wait_recv()
    lax.fori_loop(0, width // CHUNK, forward, 0)
    spreads = [spread(0, all_m)]
    cot_copies[0].wait_recv()
    partial(sib, keep(to_sib))
    near_copy = remote(5, to_sib, from_sib, send, receive, to(sib))
    near_copy.start()
    cot_copies[2].wait_recv()
    partial(diag, keep(to_sib_far))
    relay_copy = remote(6, to_sib_far, from_sib_far, send, receive, to(sib))
    relay_copy.start()
    cot_copies[1].wait_recv()
    relay_copy.wait_recv()
    partial(far, add_far)
    far_copy = remote(7, to_far, from_far, send, receive, to(far))
    far_copy.start()
    relays = []

    def relay_rows(slot, ref):
        spreads[slot][0].wait_recv()
        copy = remote(16 + slot, rows(ref, far), rows(ref, far), send, receive, to(sib))
        copy.start()
        relays.append(copy)

    relay_rows(0, all_m)
    near_copy.wait_recv()
    far_copy.wait_recv()


    def combine(at, carry):
        lanes = pl.ds(pl.multiple_of(at * CHUNK, CHUNK), CHUNK)
        taken_a, taken_v = shifted(before_a, up_a, lanes), shifted(before_v, up_v, lanes)
        total = own[:, lanes] + from_sib[:, lanes].astype(F32) + from_far[:, lanes].astype(F32)
        grad_mixed = total.astype(BF16).astype(F32)
        pre_grad_a = grad_mixed * factor[:, lanes]
        pre_grad_v = grad_mixed * gated[:, lanes]
        grad_a[:, lanes] = pre_grad_a
        grad_v[:, lanes] = pre_grad_v
        found = [jnp.sum(pre_grad_a * taken, axis=0, keepdims=True) for taken in taken_a]
        found.append(jnp.sum(pre_grad_a, axis=0, keepdims=True))
        found += [jnp.sum(pre_grad_v * taken, axis=0, keepdims=True) for taken in taken_v]
        found.append(jnp.sum(pre_grad_v, axis=0, keepdims=True))
        own_sums[:, lanes] = jnp.concatenate(found, 0)
        return carry

    lax.fori_loop(0, width // CHUNK, combine, 0)
    first = pl.ds(0, TAIL)
    back_copies = [
        remote(8, grad_a.at[first, :], after_a, send, receive, to(left)),
        remote(9, grad_v.at[first, :], after_v, send, receive, to(left)),
    ]
    sum_copies = [
        remote(19 + slot, own_sums, got_sums.at[slot], send, receive, to(peer))
        for slot, peer in enumerate((sib, far, diag))
    ]

    for copy in back_copies:
        copy.start()
    for copy in sum_copies:
        copy.start()

    def backward(grads, after, taps, out):
        def step(at, carry):
            lanes = pl.ds(pl.multiple_of(at * CHUNK, CHUNK), CHUNK)
            ext = jnp.concatenate([grads[:, lanes], after[:, lanes] * has_after], 0)
            total = jnp.zeros((length, CHUNK), F32)
            for k in range(tap_count):
                total = total + taps[k : k + 1, lanes].astype(F32) * ext[reach - k : reach - k + length]
            out[:, lanes] = total.astype(BF16)
            return carry

        lax.fori_loop(0, width // CHUNK, step, 0)

    back_copies[0].wait_recv()
    backward(grad_a, after_a, taps_a, out_a)
    spreads.append(spread(1, all_a))
    back_copies[1].wait_recv()
    backward(grad_v, after_v, taps_v, out_v)
    spreads.append(spread(2, all_v))

    def add_terms(index, pairs, fresh):
        span = pl.ds(pl.multiple_of(index * length, length), length)

        def step(at, carry):
            lanes = pl.ds(pl.multiple_of(at * CHUNK, CHUNK), CHUNK)
            total = None if fresh else terms[span, lanes]
            for ref, weights in pairs:
                product = contract_last(ref[span, :], weights[lanes, :])
                total = product if total is None else total + product
            terms[span, lanes] = total
            return carry

        lax.fori_loop(0, depth // CHUNK, step, 0)

    role_a, role_v = (all_a, held_a), (all_v, held_v)
    for load in loads:
        load.wait()
    add_terms(me, (role_a, role_v), True)
    spreads[1][1].wait_recv()
    spreads[2][1].wait_recv()
    add_terms(sib, (role_a, role_v), True)
    relay_rows(1, all_a)
    add_terms(far, (role_a,), True)
    relays[1].wait_recv()
    add_terms(diag, (role_a,), True)
    relay_rows(2, all_v)
    add_terms(far, (role_v,), False)
    relays[2].wait_recv()
    add_terms(diag, (role_v,), False)
    for copy in sum_copies:
        copy.wait_recv()
    sums[...] = (own_sums[...] + got_sums[0]) + (got_sums[1] + got_sums[2])
    spreads[0][1].wait_recv()
    relays[0].wait_recv()
    for copy in (
        *cot_copies, *halo_copies, near_copy, relay_copy, far_copy, *back_copies, *sum_copies,
        *(copy for pair in spreads for copy in pair), *relays,
    ):
        copy.wait_send()


def gradients(
    cotangent, w_down, up_act, up_val, conv_act, conv_val, bias_act, bias_val, w_act, w_val
):
    length, width = up_act.shape
    depth = w_down.shape[1]
    tp_count = lax.axis_size("tp")
    tap_count = conv_act.shape[0]
    positions = length * tp_count
    stat_rows = 2 * (tap_count + 1)
    vmem = pl.BlockSpec(memory_space=pltpu.VMEM)
    block = pltpu.VMEM((length, width), BF16)
    wide = pltpu.VMEM((length, width), F32)
    return pl.pallas_call(
        gradient_kernel,
        out_shape=(
            jax.ShapeDtypeStruct((positions, depth), BF16),
            jax.ShapeDtypeStruct((positions, width), BF16),
            jax.ShapeDtypeStruct((positions, width), BF16),
            jax.ShapeDtypeStruct((positions, width), BF16),
            jax.ShapeDtypeStruct((stat_rows, width), F32),
            jax.ShapeDtypeStruct((positions, depth), F32),
        ),
        in_specs=[vmem] * 8 + [pl.BlockSpec(memory_space=pl.ANY)] * 2,
        out_specs=(vmem,) * 6,
        scratch_shapes=[
            wide, block, block, block, block, block, block,
            pltpu.VMEM((HALO, width), BF16), pltpu.VMEM((HALO, width), BF16),
            wide, wide,
            pltpu.VMEM((TAIL, width), F32), pltpu.VMEM((TAIL, width), F32),
            pltpu.VMEM((stat_rows, width), F32), pltpu.VMEM((3, stat_rows, width), F32),
            wide, wide, pltpu.VMEM(w_act.shape, BF16), pltpu.VMEM(w_val.shape, BF16),
            pltpu.SemaphoreType.DMA((22,)), pltpu.SemaphoreType.DMA((22,)),
            pltpu.SemaphoreType.DMA((2,)),
        ],
        compiler_params=pltpu.CompilerParams(
            collective_id=0, has_side_effects=True, vmem_limit_bytes=50 * 1024 * 1024
        ),
    )(
        cotangent, w_down, up_act, up_val, conv_act, conv_val,
        bias_act.reshape(1, width), bias_val.reshape(1, width), w_act, w_val,
    )


def reduce_kernel(
    terms, stat, down_stat, out, stat_sum, down_sum,
    to_pair, from_pair, to_line, from_line, settled, got_stat, got_down,
    send, receive,
):
    fs, tp = lax.axis_index("fs"), lax.axis_index("tp")
    fs_count, tp_count = lax.axis_size("fs"), lax.axis_size("tp")
    line = fs_count // 2
    z, y = fs // 2, fs % 2
    pair = z * 2 + (1 - y)
    shard = out.shape[0]
    depth = terms.shape[1]
    length = terms.shape[0] // tp_count

    def at_fs(index):
        return {"fs": index}

    def at_tp(index):
        return {"tp": index}

    fs_others = [lax.rem(fs + by, fs_count) for by in range(1, fs_count)]
    tp_others = [lax.rem(tp + by, tp_count) for by in range(1, tp_count)]
    greet([at_fs(i) for i in fs_others] + [at_tp(i) for i in tp_others])

    def term(index):
        return jnp.concatenate(
            [
                terms[pl.ds(pl.multiple_of(part * length + index * shard, shard), shard), :]
                for part in range(tp_count)
            ],
            0,
        )

    base = 0
    steps = sorted(range(1, line), key=lambda by: -min(by, line - by)) + [0]
    there = {by: lax.rem(z + by, line) for by in steps}
    pair_copies = {}
    for by in steps:
        to_pair[by] = term(there[by] * 2 + (1 - y)).astype(BF16)
        pair_copies[by] = remote(
            base + by, to_pair.at[by], from_pair.at[by], send, receive, at_fs(pair)
        )
        pair_copies[by].start()
    base += line
    small = []
    for slot, index in enumerate(fs_others):
        small.append(remote(base + slot, stat, got_stat.at[slot], send, receive, at_fs(index)))
    base += len(fs_others)
    for slot, index in enumerate(tp_others):
        small.append(
            remote(base + slot, down_stat, got_down.at[slot], send, receive, at_tp(index))
        )
    base += len(tp_others)
    for copy in small:
        copy.start()
    line_copies = []
    total = None
    for by in steps:
        pair_copies[by].wait_recv()
        added = term(there[by] * 2 + y) + from_pair[by].astype(F32)
        if by == 0:
            total = added
        else:
            to_line[by] = added.astype(BF16)
            copy = remote(
                base + by, to_line.at[by], from_line.at[by], send, receive,
                at_fs(there[by] * 2 + y),
            )
            copy.start()
            line_copies.append((by, copy))
    base += line
    for by, copy in line_copies:
        copy.wait_recv()
        total = total + from_line[by].astype(F32)
    settled[...] = total.astype(BF16)

    def part_of(index):
        return pl.ds(pl.multiple_of(index * shard, shard), shard)

    mine = pl.ds(pl.multiple_of(tp * depth, depth), depth)
    last_copies = [
        remote(
            base + slot, settled.at[part_of(index), :], out.at[:, mine], send, receive, at_tp(index)
        )
        for slot, index in enumerate(tp_others)
    ]
    for copy in last_copies:
        copy.start()
    out[:, mine] = settled[part_of(tp), :]
    for copy in small:
        copy.wait_recv()
    stat_total = stat[...]
    for slot in range(len(fs_others)):
        stat_total = stat_total + got_stat[slot]
    stat_sum[...] = stat_total
    down_total = down_stat[...]
    for slot in range(len(tp_others)):
        down_total = down_total + got_down[slot]
    down_sum[...] = down_total
    for copy in last_copies:
        copy.wait_recv()
    for copy in (
        *pair_copies.values(), *small, *(copy for _, copy in line_copies), *last_copies,
    ):
        copy.wait_send()


def reduced(terms, stat, down_stat):
    fs_count, tp_count = lax.axis_size("fs"), lax.axis_size("tp")
    positions, depth = terms.shape
    shard = positions // (fs_count * tp_count)
    line = fs_count // 2
    vmem = pl.BlockSpec(memory_space=pltpu.VMEM)
    blocks = pltpu.VMEM((line, tp_count * shard, depth), BF16)
    copies = 2 * line + (fs_count - 1) + 2 * (tp_count - 1)
    return pl.pallas_call(
        reduce_kernel,
        out_shape=(
            jax.ShapeDtypeStruct((shard, depth * tp_count), BF16),
            jax.ShapeDtypeStruct(stat.shape, F32),
            jax.ShapeDtypeStruct(down_stat.shape, F32),
        ),
        in_specs=[vmem] * 3,
        out_specs=(vmem,) * 3,
        scratch_shapes=[
            blocks, blocks, blocks, blocks,
            pltpu.VMEM((tp_count * shard, depth), BF16),
            pltpu.VMEM((fs_count - 1,) + stat.shape, F32),
            pltpu.VMEM((tp_count - 1,) + down_stat.shape, F32),
            pltpu.SemaphoreType.DMA((copies,)), pltpu.SemaphoreType.DMA((copies,)),
        ],
        compiler_params=pltpu.CompilerParams(collective_id=1, has_side_effects=True),
    )(terms, stat, down_stat)


def kernels_fit(up_act, w_down, conv_act):
    length, width = up_act.shape
    fs_count, tp_count = lax.axis_size("fs"), lax.axis_size("tp")
    return (
        tp_count == 4
        and fs_count % 2 == 0
        and width % CHUNK == 0
        and w_down.shape[1] % CHUNK == 0
        and length % (16 * fs_count) == 0
        and conv_act.shape[0] - 1 <= TAIL
        and conv_act.shape[0] == 3
        and width * (3 * w_down.shape[1] + 32 * length) * 2 <= 32 * 1024 * 1024
    )


def weight_kernel(left, right, out, norms):
    value = contract_first(left[...], right[...])
    out[...] = value
    square = value * value
    lanes = square[:, :128]
    for at in range(128, square.shape[1], 128):
        lanes = lanes + square[:, at : at + 128]
    norms[...] = jnp.sum(lanes.T, axis=0, keepdims=True)


def weight_gradient(left, right):
    positions, height = left.shape
    width = right.shape[1]
    return pl.pallas_call(
        weight_kernel,
        grid=(height // CHUNK,),
        out_shape=(
            jax.ShapeDtypeStruct((height, width), F32),
            jax.ShapeDtypeStruct((1, height), F32),
        ),
        in_specs=[
            pl.BlockSpec((positions, CHUNK), lambda i: (0, i)),
            pl.BlockSpec((positions, width), lambda i: (0, 0)),
        ],
        out_specs=(
            pl.BlockSpec((CHUNK, width), lambda i: (i, 0)),
            pl.BlockSpec((1, CHUNK), lambda i: (0, i)),
        ),
        compiler_params=pltpu.CompilerParams(vmem_limit_bytes=40 * 1024 * 1024),
    )(left, right)


def with_kernels(
    hidden_in, up_act, up_val, cotangent, w_act, w_val, w_down,
    conv_act, conv_val, bias_act, bias_val,
):
    tap_count = conv_act.shape[0]
    cot_columns, all_up_act, all_up_val, all_mixed, sums, terms = gradients(
        cotangent, w_down, up_act, up_val, conv_act, conv_val, bias_act, bias_val, w_act, w_val
    )
    grad_w_act, act_norms = weight_gradient(hidden_in, all_up_act)
    grad_w_val, val_norms = weight_gradient(hidden_in, all_up_val)
    grad_w_down, down_norms = weight_gradient(all_mixed, cot_columns)
    taps_act, sums_act = sums[:tap_count], sums[tap_count]
    taps_val, sums_val = sums[tap_count + 1 : 2 * tap_count + 1], sums[2 * tap_count + 1]
    tap_squares = jnp.stack(
        [jnp.sum(taps_act * taps_act, axis=1), jnp.sum(taps_val * taps_val, axis=1)], 0
    )
    depth = hidden_in.shape[1]
    flat = tap_squares.reshape(1, -1)
    stat = jnp.concatenate(
        [
            act_norms,
            val_norms,
            jnp.pad(flat, ((0, 0), (0, depth - flat.shape[1]))),
            jnp.zeros((5, depth), F32),
        ],
        0,
    )
    down_stat = jnp.pad(down_norms, ((0, 7), (0, 0)))
    grad_input, stat, down_stat = reduced(terms, stat, down_stat)
    return (
        grad_input,
        grad_w_act,
        grad_w_val,
        grad_w_down,
        taps_act,
        taps_val,
        sums_act,
        sums_val,
        stat[0],
        stat[1],
        down_stat[0],
        stat[2, : 2 * tap_count].reshape(2, tap_count),
    )


def passed_along(value, axis, by):
    length = lax.axis_size(axis)
    pairs = [(i, i + by) for i in range(length) if 0 <= i + by < length]
    return lax.ppermute(value, axis, pairs)


def contract_last(left, right):
    return lax.dot_general(
        left, right, (((1,), (1,)), ((), ())), preferred_element_type=jnp.float32
    )


def contract_first(left, right):
    return lax.dot_general(
        left, right, (((0,), (0,)), ((), ())), preferred_element_type=jnp.float32
    )


def conv_ahead(extended, taps, bias, length):
    total = jnp.zeros((length, extended.shape[1]), jnp.float32) + bias.astype(jnp.float32)
    for offset in range(taps.shape[0]):
        total = total + taps[offset].astype(jnp.float32) * extended[offset : offset + length]
    return total


def conv_behind(extended, taps, length):
    reach = taps.shape[0] - 1
    total = jnp.zeros((length, extended.shape[1]), jnp.float32)
    for offset in range(taps.shape[0]):
        total = (
            total
            + taps[offset].astype(jnp.float32) * extended[reach - offset : reach - offset + length]
        )
    return total.astype(jnp.bfloat16)


def tap_grads(grad_pre, extended, tap_count):
    length = grad_pre.shape[0]
    rows = [
        jnp.sum(grad_pre * extended[offset : offset + length], axis=0)
        for offset in range(tap_count)
    ]
    return (jnp.stack(rows, 0), jnp.sum(grad_pre, axis=0))


def per_device(
    hidden_in,
    up_act,
    up_val,
    cotangent,
    w_act,
    w_val,
    w_down,
    conv_act,
    conv_val,
    bias_act,
    bias_val,
):
    if kernels_fit(up_act, w_down, conv_act):
        return with_kernels(
            hidden_in, up_act, up_val, cotangent, w_act, w_val, w_down,
            conv_act, conv_val, bias_act, bias_val,
        )
    local_rows = cotangent.shape[0]
    tap_count = conv_act.shape[0]
    reach = tap_count - 1
    tp_count = lax.axis_size("tp")
    fs_count = lax.axis_size("fs")
    down_whole = lax.all_gather(w_down, "tp", axis=1, tiled=True)
    prev_act, prev_val = passed_along(
        (up_act[local_rows - reach :], up_val[local_rows - reach :]), "tp", 1
    )
    ext_act = jnp.concatenate([prev_act, up_act], 0).astype(jnp.float32)
    ext_val = jnp.concatenate([prev_val, up_val], 0).astype(jnp.float32)
    pre_act = conv_ahead(ext_act, conv_act, bias_act, local_rows)
    pre_val = conv_ahead(ext_val, conv_val, bias_val, local_rows)
    gelu_act, gelu_back = jax.vjp(jax.nn.gelu, pre_act)
    mixed = (gelu_act * pre_val).astype(jnp.bfloat16)
    grad_mixed = contract_last(cotangent, down_whole).astype(jnp.bfloat16)
    grad_mixed = lax.optimization_barrier(grad_mixed).astype(jnp.float32)
    grad_pre_act = gelu_back(grad_mixed * pre_val)[0]
    grad_pre_val = grad_mixed * gelu_act
    next_act, next_val = passed_along((grad_pre_act[:reach], grad_pre_val[:reach]), "tp", -1)
    grad_up_act = conv_behind(jnp.concatenate([grad_pre_act, next_act], 0), conv_act, local_rows)
    grad_up_val = conv_behind(jnp.concatenate([grad_pre_val, next_val], 0), conv_val, local_rows)
    taps_act, sums_act = tap_grads(grad_pre_act, ext_act, tap_count)
    taps_val, sums_val = tap_grads(grad_pre_val, ext_val, tap_count)
    all_up_act, all_up_val, all_mixed = (
        lax.all_gather(grad_up_act, "tp", axis=0, tiled=True),
        lax.all_gather(grad_up_val, "tp", axis=0, tiled=True),
        lax.all_gather(mixed, "tp", axis=0, tiled=True),
    )
    cot_columns = lax.all_to_all(cotangent, "tp", split_axis=1, concat_axis=0, tiled=True)
    grad_w_act = contract_first(hidden_in, all_up_act)
    grad_w_val = contract_first(hidden_in, all_up_val)
    grad_w_down = contract_first(all_mixed, cot_columns)
    shard_rows = local_rows // fs_count
    block_rows = tp_count * shard_rows

    def select_rows(gathered):
        shaped = gathered.reshape(tp_count, fs_count, shard_rows, gathered.shape[1])
        return jnp.transpose(shaped, (1, 0, 2, 3)).reshape(
            lax.axis_size("fs") * block_rows, gathered.shape[1]
        )

    summed = lax.psum_scatter(
        contract_last(select_rows(all_up_act), w_act)
        + contract_last(select_rows(all_up_val), w_val),
        "fs",
        scatter_dimension=0,
        tiled=True,
    ).astype(jnp.bfloat16)
    grad_input = lax.all_to_all(summed, "tp", split_axis=0, concat_axis=1, tiled=True)
    down_squares = jnp.sum(grad_w_down * grad_w_down, axis=1)
    taps_act, taps_val, sums_act, sums_val, rows_down = lax.psum(
        (taps_act, taps_val, sums_act, sums_val, down_squares), "tp"
    )
    tap_squares = jnp.stack(
        [jnp.sum(taps_act * taps_act, axis=1), jnp.sum(taps_val * taps_val, axis=1)], 0
    )
    rows_act, rows_val, conv_rows = lax.psum(
        (
            jnp.sum(grad_w_act * grad_w_act, axis=1),
            jnp.sum(grad_w_val * grad_w_val, axis=1),
            tap_squares,
        ),
        "fs",
    )
    return (
        grad_input,
        grad_w_act,
        grad_w_val,
        grad_w_down,
        taps_act,
        taps_val,
        sums_act,
        sums_val,
        rows_act,
        rows_val,
        rows_down,
        conv_rows,
    )


def solution(mesh):
    return jax.shard_map(
        per_device,
        mesh=mesh,
        in_specs=(
            P(None, "tp"),
            P("tp", "fs"),
            P("tp", "fs"),
            P("tp", None),
            P("tp", "fs"),
            P("tp", "fs"),
            P("fs", "tp"),
            P(None, "fs"),
            P(None, "fs"),
            P("fs"),
            P("fs"),
        ),
        out_specs=(
            P(("tp", "fs"), None),
            P("tp", "fs"),
            P("tp", "fs"),
            P("fs", "tp"),
            P(None, "fs"),
            P(None, "fs"),
            P("fs"),
            P("fs"),
            P("tp"),
            P("tp"),
            P("fs"),
            P(),
        ),
        check_vma=False,
    )
```

profile of v0, /device:TPU:0, one launch (start us, length us, event | category | flops | bytes accessed | tf_op | source)
XLA Modules:
  0.0 126.7 jit_solution(7074540574220929578)
XLA Ops:
  0.7 0.1 pad.13.clone
  0.7 0.7 reshape.33.bias_a
  1.4 0.7 reshape.34.bias_v
  2.1 0.0 copy-start.4
  2.1 1.2 copy-done.4
  3.3 0.0 copy-start.7
  3.3 1.0 copy-done.7
  4.3 0.0 copy-start.8
  4.3 1.0 copy-done.8
  5.3 0.0 copy-start.9
  5.3 0.7 copy-done.9
  6.0 0.0 copy-start.10
  6.0 0.7 copy-done.10
  6.7 0.0 copy-start
  6.7 65.2 %shard_map.202 = (bf16[512,1024]{1,0:T(8,128)(2,1)S(1)}, bf16[512,1536]{1,0:T(8,128)(2,1)}, bf16[512,1536]{1,0:T(8,128)(2,1)}, bf16[512,1536]{1,0:T(8,128)(2,1)}...) custom-call(bf16[128,4096]{1,0:T(8,128)(2,1)S(1)} %copy-done.4, bf16[1536,1024]{1,0:T(8,128)(2,1)} %down.1, ...), custom_call_target="tpu_custom_call" | custom-call | tf_op jit(solution)/shard_map/pallas_call | solution.py:278
  71.9 0.0 copy-start.5
  71.9 1.0 copy-done.5
  72.9 0.0 copy-start.1
  72.9 0.8 multiply_reduce_fusion.1
  73.7 0.1 reshape.35
  73.7 0.0 copy-done
  73.8 0.0 copy-start.3
  73.8 1.4 %copy-done.3 = bf16[512,1536]{1,0:T(8,128)(2,1)S(1)} copy-done((bf16[512,1536]{1,0:T(8,128)(2,1)S(1)}, bf16[512,1536]{1,0:T(8,128)(2,1)}, u32[]{:S(2)}) %copy-start.3) | copy-done | bytes 1572888
  75.2 0.0 copy-start.6
  75.2 4.3 %shard_map.203 = (f32[1024,1536]{1,0:T(8,128)}, f32[1,1024]{1,0:T(1,128)S(1)}) custom-call(bf16[512,1024]{1,0:T(8,128)(2,1)S(1)} %copy-done, bf16[512,1536]{1,0:T(8,128)(2,1)S(1)} %copy-done.3), custom_call_target="tpu_custom_call" | custom-call | tf_op jit(solution)/shard_map/pallas_call | solution.py:472
  79.5 0.0 copy-start.2
  79.5 1.4 %copy-done.2 = bf16[512,1536]{1,0:T(8,128)(2,1)S(1)} copy-done((bf16[512,1536]{1,0:T(8,128)(2,1)S(1)}, bf16[512,1536]{1,0:T(8,128)(2,1)}, u32[]{:S(2)}) %copy-start.2) | copy-done | bytes 1572888
  80.9 4.3 %shard_map.204 = (f32[1024,1536]{1,0:T(8,128)}, f32[1,1024]{1,0:T(1,128)S(1)}) custom-call(bf16[512,1024]{1,0:T(8,128)(2,1)S(1)} %copy-done, bf16[512,1536]{1,0:T(8,128)(2,1)S(1)} %copy-done.2), custom_call_target="tpu_custom_call" | custom-call | tf_op jit(solution)/shard_map/pallas_call | solution.py:472
  85.1 0.7 fusion.stat
  85.8 0.0 copy-done.1
  85.8 0.0 copy-done.6
  85.8 4.9 %shard_map.205 = (f32[1536,1024]{1,0:T(8,128)}, f32[1,1536]{1,0:T(1,128)S(1)}) custom-call(bf16[512,1536]{1,0:T(8,128)(2,1)S(1)} %copy-done.1, bf16[512,1024]{1,0:T(8,128)(2,1)S(1)} %copy-done.6), custom_call_target="tpu_custom_call" | custom-call | tf_op jit(solution)/shard_map/pallas_call | solution.py:472
  90.8 0.6 pad.9.down_stat
  91.4 29.5 %shard_map.206 = (bf16[16,4096]{1,0:T(8,128)(2,1)}, f32[8,1024]{1,0:T(8,128)}, f32[8,1536]{1,0:T(8,128)}) custom-call(f32[512,1024]{1,0:T(8,128)} %get-tuple-element.27.terms, f32[8,1024]{1,0:T(8,128)} %fusion.stat, f32[8,1536]{1,0:T(8,128)} %pad.9.down_stat), custom_call_target="tpu_custom_call" | custom-call | tf_op jit(solution)/shard_map/pallas_call | solution.py:424
  120.9 1.5 %slice_reduce_fusion.1 = (f32[1536]{0:T(1024)}, f32[1536]{0:T(1024)}, f32[1536]{0:T(1024)}) fusion(f32[8,1536]{1,0:T(8,128)S(1)} %get-tuple-element.32, f32[8,1536]{1,0:T(8,128)} %get-tuple-element.41), kind=kLoop, calls=%fused_computation.8 | loop fusion | bytes 36864 | tf_op jit(solution)/shard_map/slice | solution.py:503
  122.3 0.7 slice_reduce_fusion.3
  123.0 1.4 %fusion.2 = (f32[1,1024]{1,0:T(1,128)}, f32[1,1024]{1,0:T(1,128)}) fusion(f32[8,1024]{1,0:T(8,128)} %get-tuple-element.40), kind=kLoop, calls=%fused_computation.12 | loop fusion | bytes 16384 | tf_op jit(solution)/shard_map/slice | solution.py:530
  124.5 0.6 reshape_squeeze.3
  125.1 1.6 %copy.24 = bf16[16,4096]{1,0:T(8,128)(2,1)} copy(bf16[16,4096]{1,0:T(8,128)(2,1)} %get-tuple-element.65) | data formatting | bytes 262144
  (2 shorter events, 0.0 us)
Async XLA Ops:
  2.1 1.2 copy-start.4
  3.3 1.0 copy-start.7
  4.3 1.0 copy-start.8
  5.3 0.7 copy-start.9
  6.0 0.7 copy-start.10
  6.7 67.0 %copy-start = (bf16[512,1024]{1,0:T(8,128)(2,1)S(1)}, bf16[512,1024]{1,0:T(8,128)(2,1)}, u32[]{:S(2)}) copy-start(bf16[512,1024]{1,0:T(8,128)(2,1)} %left.3) | copy-start | bytes 3145732
  71.9 1.0 copy-start.5
  72.9 12.9 %copy-start.1 = (bf16[512,1536]{1,0:T(8,128)(2,1)S(1)}, bf16[512,1536]{1,0:T(8,128)(2,1)}, u32[]{:S(2)}) copy-start(bf16[512,1536]{1,0:T(8,128)(2,1)} %get-tuple-element.33.left) | copy-start | bytes 4718596
  73.8 1.4 %copy-start.3 = (bf16[512,1536]{1,0:T(8,128)(2,1)S(1)}, bf16[512,1536]{1,0:T(8,128)(2,1)}, u32[]{:S(2)}) copy-start(bf16[512,1536]{1,0:T(8,128)(2,1)} %get-tuple-element.28.right) | copy-start | bytes 4718596
  75.2 10.7 %copy-start.6 = (bf16[512,1024]{1,0:T(8,128)(2,1)S(1)}, bf16[512,1024]{1,0:T(8,128)(2,1)}, u32[]{:S(2)}) copy-start(bf16[512,1024]{1,0:T(8,128)(2,1)} %copy-done.5) | copy-start | bytes 3145732
  79.5 1.4 %copy-start.2 = (bf16[512,1536]{1,0:T(8,128)(2,1)S(1)}, bf16[512,1536]{1,0:T(8,128)(2,1)}, u32[]{:S(2)}) copy-start(bf16[512,1536]{1,0:T(8,128)(2,1)} %get-tuple-element.30.right) | copy-start | bytes 4718596
where the time goes:
time: 127 us
  Pallas kernels  108 us (85%)
  local copies, waits for them, and re-layouts  16.4 us (13%)
  other arithmetic  1.45 us (1%)
    pallas_call x1, Pallas kernels, gradients(): pl.pallas_call(gradient_kernel, out_shape=(jax.ShapeDtypeStruct((position...  65.2 us
    pallas_call x1, Pallas kernels, reduced(): pl.pallas_call(reduce_kernel, out_shape=(jax.ShapeDtypeStruct((shard, dep...  29.5 us
    pallas_call x3, Pallas kernels, weight_gradient(): pl.pallas_call(weight_kernel, grid=(height // CHUNK,), out_shape=(jax.Sha...  13.5 us
    unnamed x23, local copies, waits for them, and re-layouts  9.99 us

commit v1 on v0

v1 whole, which is shorter than its diff:
```python
import itertools

import jax
import jax.numpy as jnp
from jax import lax
from jax.experimental import pallas as pl
from jax.experimental.pallas import tpu as pltpu
from jax.sharding import PartitionSpec as P

MESH = pl.DeviceIdType.MESH
F32 = jnp.float32
BF16 = jnp.bfloat16
CHUNK = 256
GROUP = 512
HALO = 16
TAIL = 8
COPIES = 112
ROOT_TWO_OVER_PI = 0.7978845608028654
CUBIC = 0.044715


def span(index, size):
    return pl.ds(pl.multiple_of(index * size, size), size)


def gradient_kernel(
    hidden_hbm, up_a_hbm, up_v_hbm, cot_hbm, w_a_hbm, w_v_hbm, down_hbm, params,
    columns, all_g, all_m, sums, out, norms, down_norms, squares,
    hidden, up, cot, weights, down,
    before, after, grads, gated, factor,
    own, to_sib, from_sib, to_sib_far, from_sib_far, to_far, from_far,
    terms, to_pair, from_pair, kept, to_line, from_line, settled,
    own_sums, sib_sums, chip_sums, far_sums, own_norms, got_norms, own_down, got_down,
    own_squares, got_squares,
    send, receive, loaded,
):
    me, fs = lax.axis_index("tp"), lax.axis_index("fs")
    count, fs_count = lax.axis_size("tp"), lax.axis_size("fs")
    chip, core = me // 2, me % 2
    other = 1 - chip
    sib, far, diag = chip * 2 + (1 - core), other * 2 + core, other * 2 + (1 - core)
    line = fs_count // 2
    z, y = fs // 2, fs % 2
    pair = z * 2 + (1 - y)
    z_mate = z + 1 - 2 * (z % 2)
    length, width = up.shape[1:]
    depth = down.shape[1]
    tap_count = params.shape[0] // 2 - 1
    reach = tap_count - 1
    group_count = width // GROUP
    shard = out.shape[0]
    quarter = length // 4

    def to(index):
        return {"tp": index}

    def to_fs(index):
        return {"fs": index}

    fs_others = [lax.rem(fs + by, fs_count) for by in range(1, fs_count)]
    numbers = itertools.count()
    pending = []

    def copy_of(source, target, where, send_at=None, receive_at=None):
        number = next(numbers) if send_at is None else send_at
        assert number < COPIES
        return pltpu.make_async_remote_copy(
            src_ref=source,
            dst_ref=target,
            send_sem=send.at[number],
            recv_sem=receive.at[number if receive_at is None else receive_at],
            device_id=where,
            device_id_type=MESH,
        )

    def launch(source, target, where):
        copy = copy_of(source, target, where)
        copy.start()
        pending.append(copy)
        return copy

    def rows(index):
        return span(index, length)

    def cols(index):
        return span(index, depth)

    def group(g):
        return pl.ds(g * GROUP, GROUP)

    def chunks(g, step):
        def at(i, carry):
            step(pl.ds(pl.multiple_of(g * GROUP + i * CHUNK, CHUNK), CHUNK))
            return carry

        lax.fori_loop(0, GROUP // CHUNK, at, 0)

    def depth_chunks(step):
        def at(i, carry):
            step(span(i, CHUNK))
            return carry

        lax.fori_loop(0, depth // CHUNK, at, 0)

    sources = (
        (up_a_hbm, up.at[0]), (up_v_hbm, up.at[1]), (cot_hbm, cot), (down_hbm, down),
        (hidden_hbm, hidden), (w_a_hbm, weights.at[0]), (w_v_hbm, weights.at[1]),
    )
    loads = [
        pltpu.make_async_copy(source, target, loaded.at[i])
        for i, (source, target) in enumerate(sources)
    ]
    for load in loads:
        load.start()

    barrier = pltpu.get_barrier_semaphore()
    everyone = [to(sib), to(far), to(diag)] + [to_fs(index) for index in fs_others]
    for where in everyone:
        pl.semaphore_signal(barrier, inc=1, device_id=where, device_id_type=MESH)
    pl.semaphore_wait(barrier, len(everyone))

    loads[0].wait()
    loads[1].wait()
    has_before, has_after = me > 0, me < count - 1
    last = pl.ds(length - HALO, HALO)
    halo = [copy_of(up.at[r, last, :], before.at[r], to(lax.rem(me + 1, count))) for r in range(2)]

    @pl.when(has_after)
    def _():
        for copy in halo:
            copy.start()

    @pl.when(jnp.logical_not(has_before))
    def _():
        before[...] = jnp.zeros(before.shape, before.dtype)

    @pl.when(jnp.logical_not(has_after))
    def _():
        after[...] = jnp.zeros(after.shape, after.dtype)

    loads[2].wait()
    mine = span((z % 2) * 2 + y, quarter)

    def quarter_of(index):
        at = index * length + ((z % 2) * 2 + y) * quarter
        return columns.at[pl.ds(pl.multiple_of(at, quarter), quarter), :]

    cot_far = launch(cot.at[mine, cols(far)], quarter_of(me), to(far))
    cot_diag = launch(cot.at[mine, cols(diag)], quarter_of(me), to(diag))
    cot_sib = launch(cot.at[:, cols(sib)], columns.at[rows(me), :], to(sib))
    columns[rows(me), :] = cot[:, cols(me)]

    def share(index):
        mates = (pair, z_mate * 2 + y, z_mate * 2 + (1 - y))
        return [launch(quarter_of(index), quarter_of(index), to_fs(mate)) for mate in mates]

    def shifted(r, lanes):
        ext = jnp.concatenate([before[r, :, lanes].astype(F32), up[r, :, lanes].astype(F32)], 0)
        return [ext[HALO - reach + k : HALO - reach + k + length] for k in range(tap_count)]

    def param(r, k, lanes):
        at = r * (tap_count + 1) + k
        return params[at : at + 1, lanes]

    def forward(lanes):
        pre = []
        for r in range(2):
            taken = shifted(r, lanes)
            total = jnp.broadcast_to(param(r, tap_count, lanes), (length, CHUNK))
            for k in range(tap_count):
                total = total + param(r, k, lanes) * taken[k]
            pre.append(total)
        pre_a, pre_v = pre
        square = pre_a * pre_a
        bent = jnp.tanh(ROOT_TWO_OVER_PI * pre_a * (1.0 + CUBIC * square))
        half = 0.5 * (1.0 + bent)
        gelu = pre_a * half
        slope = half + 0.5 * pre_a * (1.0 - bent * bent) * (
            ROOT_TWO_OVER_PI * (1.0 + 3.0 * CUBIC * square)
        )
        all_m[rows(me), lanes] = (gelu * pre_v).astype(BF16)
        gated[:, lanes] = gelu
        factor[:, lanes] = pre_v * slope

    mixed_far, mixed_sib = [], []

    def spread_mixed(g):
        here = all_m.at[rows(me), group(g)]
        mixed_far.append(launch(here, here, to(far)))
        mixed_sib.append(launch(here, here, to(sib)))

    @pl.when(has_before)
    def _():
        for copy in halo:
            copy.wait_recv()

    shares = []
    for g in range(group_count):
        chunks(g, forward)
        spread_mixed(g)
        if g == 0:
            cot_far.wait_recv()
            shares += share(far)
        if g == 1:
            cot_diag.wait_recv()
            shares += share(diag)

    loads[3].wait()

    def partial(index, g, finish):
        def step(lanes):
            finish(lanes, contract_last(columns[rows(index), :], down[lanes, :]))

        chunks(g, step)

    def keep(target):
        def finish(lanes, value):
            target[:, lanes] = value.astype(target.dtype)

        return finish

    def add_far(lanes, value):
        to_far[:, lanes] = (value + from_sib_far[:, lanes].astype(F32)).astype(BF16)

    for g in range(group_count):
        partial(me, g, keep(own))
    cot_sib.wait_recv()
    for g in range(group_count):
        partial(sib, g, keep(to_sib))
    near = launch(to_sib, from_sib, to(sib))
    for copy in shares:
        copy.wait_recv()

    relayed, crossed = [], []

    def diag_part(g):
        partial(diag, g, keep(to_sib_far))
        relayed.append(launch(to_sib_far.at[:, group(g)], from_sib_far.at[:, group(g)], to(sib)))

    def far_part(g):
        relayed[g].wait_recv()
        partial(far, g, add_far)
        crossed.append(launch(to_far.at[:, group(g)], from_far.at[:, group(g)], to(far)))

    diag_part(0)
    for g in range(1, group_count):
        diag_part(g)
        far_part(g - 1)
    far_part(group_count - 1)

    mixed_relays = []

    def relay_mixed(g):
        mixed_far[g].wait_recv()
        there = all_m.at[rows(far), group(g)]
        mixed_relays.append(launch(there, there, to(sib)))

    def combine(lanes):
        total = own[:, lanes] + from_sib[:, lanes].astype(F32) + from_far[:, lanes].astype(F32)
        grad_mixed = total.astype(BF16).astype(F32)
        for r, scale in ((0, factor), (1, gated)):
            pre_grad = grad_mixed * scale[:, lanes]
            grads[r, :, lanes] = pre_grad
            found = [
                jnp.sum(pre_grad * taken, axis=0, keepdims=True) for taken in shifted(r, lanes)
            ]
            found.append(jnp.sum(pre_grad, axis=0, keepdims=True))
            own_sums[r, :, lanes] = jnp.concatenate(found, 0)

    def backward(lanes):
        for r in range(2):
            ext = jnp.concatenate([grads[r, :, lanes], after[r, :, lanes]], 0)
            total = jnp.zeros((length, CHUNK), F32)
            for k in range(tap_count):
                total = total + param(r, k, lanes) * ext[reach - k : reach - k + length]
            all_g[r, rows(me), lanes] = total.astype(BF16)

    first = pl.ds(0, TAIL)
    left = lax.rem(me + count - 1, count)
    backs, sent_g = [], []
    near.wait_recv()
    for g in range(group_count):
        crossed[g].wait_recv()
        chunks(g, combine)
        back = [
            copy_of(grads.at[r, first, group(g)], after.at[r, :, group(g)], to(left))
            for r in range(2)
        ]
        backs += back

        @pl.when(has_before)
        def _():
            for copy in back:
                copy.start()

        if g == 0:
            for early in range(group_count - 1):
                relay_mixed(early)

        @pl.when(has_after)
        def _():
            for copy in back:
                copy.wait_recv()

        chunks(g, backward)
        beside = []
        for r in range(2):
            here = all_g.at[r, rows(me), group(g)]
            beside.append(launch(here, here, to(sib)))
        for copy in beside:
            copy.wait_recv()
        for j in range(2):
            here = all_g.at[core, rows(chip * 2 + j), group(g)]
            sent_g.append(launch(here, here, to(far)))
    relay_mixed(group_count - 1)
    side_sums = launch(own_sums.at[1 - core], sib_sums, to(sib))

    loads[5].wait()
    loads[6].wait()

    def product(at, lanes, ks):
        total = contract_last(all_g[0, at, ks], weights[0, lanes, ks])
        return total + contract_last(all_g[1, at, ks], weights[1, lanes, ks])

    both = span(chip, 2 * length)
    depth_chunks(lambda lanes: terms.__setitem__(
        (both, lanes), product(both, lanes, pl.ds(0, width))
    ))

    blocks = (me, sib, other * 2, other * 2 + 1)

    def slab(k, index):
        return pl.ds(pl.multiple_of(blocks[k] * length + index * shard, shard), shard)

    pair_copies, line_copies, last_copies = {}, {}, {}

    def send_pair(k):
        for there in range(line):
            to_pair[k, there * shard : (there + 1) * shard, :] = terms[
                slab(k, there * 2 + (1 - y)), :
            ].astype(BF16)
        pair_copies[k] = launch(to_pair.at[k], from_pair.at[k], to_fs(pair))

    def send_line(k):
        pair_copies[k].wait_recv()
        line_copies[k] = []
        for by in sorted(range(1, line), key=lambda by: -min(by, line - by)) + [0]:
            there = lax.rem(z + by, line)
            added = terms[slab(k, there * 2 + y), :] + from_pair[
                k, span(there, shard), :
            ].astype(F32)
            if by == 0:
                kept[k] = added
            else:
                to_line[k, by] = added.astype(BF16)
                line_copies[k].append(
                    (by, launch(to_line.at[k, by], from_line.at[k, by], to_fs(there * 2 + y)))
                )

    a2a = [next(numbers) for _ in range(2)]

    def settle(k):
        total = kept[k]
        for by, copy in line_copies[k]:
            copy.wait_recv()
            total = total + from_line[k, by].astype(F32)
        if k == 0:
            out[:, cols(me)] = total.astype(BF16)
            return
        settled[k] = total.astype(BF16)
        if k == 1:
            last_copies[k] = launch(settled.at[k], out.at[:, cols(me)], to(sib))
        else:
            last_copies[k] = copy_of(
                settled.at[k], out.at[:, cols(me)], to(blocks[k]),
                send_at=a2a[k - 2], receive_at=a2a[0] + core,
            )
            last_copies[k].start()
            pending.append(last_copies[k])

    send_pair(0)
    send_pair(1)

    for copy in mixed_sib:
        copy.wait_recv()
    for copy in mixed_relays:
        copy.wait_recv()
    loads[4].wait()
    own_down[...] = jnp.zeros(own_down.shape, F32)

    def down_step(lanes):
        value = contract_first(columns[:, lanes], all_m[...])
        own_down[...] += jnp.sum(value * value, axis=0, keepdims=True)

    depth_chunks(down_step)
    got_down[me] = own_down[...]
    tp_others = [lax.rem(me + by, count) for by in range(1, count)]
    down_copies = [launch(own_down, got_down.at[me], to(index)) for index in tp_others]

    side_sums.wait_recv()
    chip_sums[...] = own_sums[core] + sib_sums[...]
    cross_sums = launch(chip_sums, far_sums, to(far))
    send_line(0)
    send_line(1)

    own_norms[...] = jnp.zeros(own_norms.shape, F32)

    def norm_group(g):
        def step(lanes):
            for r in range(2):
                value = contract_first(all_g[r, :, lanes], hidden[...])
                own_norms[r : r + 1, :] += jnp.sum(value * value, axis=0, keepdims=True)

        chunks(g, step)

    theirs = span(other, 2 * length)

    def relay_g(g, j):
        sent_g[2 * g + j].wait_recv()
        there = all_g.at[core, rows(other * 2 + j), group(g)]
        return launch(there, there, to(sib))

    for g in range(group_count - 1):
        relays = [relay_g(g, j) for j in range(2)]
        for copy in relays:
            copy.wait_recv()

        def add_group(lanes):
            value = product(theirs, lanes, group(g))
            terms[theirs, lanes] = value if g == 0 else terms[theirs, lanes] + value

        depth_chunks(add_group)
        if g == 0:
            cross_sums.wait_recv()
            sums[core] = chip_sums[...] + far_sums[...]
            side_total = launch(sums.at[core], sums.at[core], to(sib))
            settle(0)
            settle(1)
        norm_group(g)

    side_total.wait_recv()
    total_sums = sums[...]
    own_squares[...] = jnp.broadcast_to(
        jnp.sum(total_sums * total_sums, axis=2, keepdims=True), own_squares.shape
    )
    got_squares[fs] = own_squares[...]
    square_copies = [launch(own_squares, got_squares.at[fs], to_fs(index)) for index in fs_others]

    g = group_count - 1
    for j in range(2):
        relay_g(g, j).wait_recv()
        at = rows(other * 2 + j)

        def add_last(lanes):
            value = product(at, lanes, group(g))
            terms[at, lanes] = value if g == 0 else terms[at, lanes] + value

        depth_chunks(add_last)
        send_pair(2 + j)
    norm_group(g)
    got_norms[fs] = own_norms[...]
    norm_copies = [launch(own_norms, got_norms.at[fs], to_fs(index)) for index in fs_others]
    send_line(2)
    send_line(3)
    settle(2)
    settle(3)
    for copies in (down_copies, square_copies, norm_copies):
        for copy in copies:
            copy.wait_recv()

    def gathered(ref, size):
        total = ref[0]
        for index in range(1, size):
            total = total + ref[index]
        return total

    down_norms[...] = gathered(got_down, count)
    squares[...] = gathered(got_squares, fs_count)
    norms[...] = gathered(got_norms, fs_count)
    last_copies[1].wait_recv()
    for j in range(2):
        copy_of(
            settled.at[0], out.at[:, cols(other * 2 + j)], to(far),
            send_at=a2a[0], receive_at=a2a[j],
        ).wait_recv()
    for copy in pending:
        copy.wait_send()

    @pl.when(has_after)
    def _():
        for copy in halo:
            copy.wait_send()

    @pl.when(has_before)
    def _():
        for copy in backs:
            copy.wait_send()


def gradients(hidden_in, up_act, up_val, cotangent, w_act, w_val, w_down, params):
    length, width = up_act.shape
    depth = w_down.shape[1]
    tp_count, fs_count = lax.axis_size("tp"), lax.axis_size("fs")
    positions = length * tp_count
    shard = length // fs_count
    line = fs_count // 2
    stat_rows = params.shape[0] // 2
    vmem = pl.BlockSpec(memory_space=pltpu.VMEM)
    hbm = pl.BlockSpec(memory_space=pl.ANY)
    block = pltpu.VMEM((length, width), BF16)
    wide = pltpu.VMEM((length, width), F32)
    slots = pltpu.VMEM((4, line * shard, depth), BF16)
    pieces = pltpu.VMEM((4, line, shard, depth), BF16)
    half_sums = pltpu.VMEM((stat_rows, width), F32)
    return pl.pallas_call(
        gradient_kernel,
        out_shape=(
            jax.ShapeDtypeStruct((positions, depth), BF16),
            jax.ShapeDtypeStruct((2, positions, width), BF16),
            jax.ShapeDtypeStruct((positions, width), BF16),
            jax.ShapeDtypeStruct((2, stat_rows, width), F32),
            jax.ShapeDtypeStruct((shard, depth * tp_count), BF16),
            jax.ShapeDtypeStruct((2, depth), F32),
            jax.ShapeDtypeStruct((1, width), F32),
            jax.ShapeDtypeStruct((2, stat_rows, 128), F32),
        ),
        in_specs=[hbm] * 7 + [vmem],
        out_specs=(vmem,) * 8,
        scratch_shapes=[
            pltpu.VMEM(hidden_in.shape, BF16),
            pltpu.VMEM((2, length, width), BF16),
            pltpu.VMEM(cotangent.shape, BF16),
            pltpu.VMEM((2,) + w_act.shape, BF16),
            pltpu.VMEM(w_down.shape, BF16),
            pltpu.VMEM((2, HALO, width), BF16), pltpu.VMEM((2, TAIL, width), F32),
            pltpu.VMEM((2, length, width), F32), wide, wide,
            wide, block, block, block, block, block, block,
            pltpu.VMEM((positions, depth), F32),
            slots, slots, pltpu.VMEM((4, shard, depth), F32), pieces, pieces,
            pltpu.VMEM((4, shard, depth), BF16),
            pltpu.VMEM((2, stat_rows, width), F32), half_sums, half_sums, half_sums,
            pltpu.VMEM((2, depth), F32), pltpu.VMEM((fs_count, 2, depth), F32),
            pltpu.VMEM((1, width), F32), pltpu.VMEM((tp_count, 1, width), F32),
            pltpu.VMEM((2, stat_rows, 128), F32), pltpu.VMEM((fs_count, 2, stat_rows, 128), F32),
            pltpu.SemaphoreType.DMA((COPIES,)), pltpu.SemaphoreType.DMA((COPIES,)),
            pltpu.SemaphoreType.DMA((7,)),
        ],
        compiler_params=pltpu.CompilerParams(
            collective_id=0, has_side_effects=True, vmem_limit_bytes=50 * 1024 * 1024
        ),
    )(hidden_in, up_act, up_val, cotangent, w_act, w_val, w_down, params)


def kernels_fit(up_act, w_down, conv_act):
    length, width = up_act.shape
    fs_count, tp_count = lax.axis_size("fs"), lax.axis_size("tp")
    return (
        tp_count == 4
        and fs_count % 4 == 0
        and width % GROUP == 0
        and width // GROUP > 1
        and w_down.shape[1] % CHUNK == 0
        and length % (16 * fs_count) == 0
        and conv_act.shape[0] - 1 <= TAIL
        and conv_act.shape[0] == 3
        and width * (3 * w_down.shape[1] + 32 * length) * 2 <= 32 * 1024 * 1024
    )


def weight_kernel(
    hidden, all_g, all_m, columns, sums, grad_in, norms, down_norms, squares,
    w_act, w_val, w_down, input_out, conv_a, conv_v, bias_a, bias_v,
    rows_a, rows_v, rows_d, conv_rows,
):
    step = pl.program_id(0)
    per_role = pl.num_programs(0) - all_m.shape[1] // CHUNK
    per_role = per_role // 2
    taps = conv_a.shape[0]

    @pl.when(step < per_role)
    def _():
        w_act[...] = contract_first(hidden[:, span(step, CHUNK)], all_g[0])

    @pl.when(jnp.logical_and(step >= per_role, step < 2 * per_role))
    def _():
        w_val[...] = contract_first(hidden[:, span(step - per_role, CHUNK)], all_g[1])

    @pl.when(step >= 2 * per_role)
    def _():
        w_down[...] = contract_first(all_m[:, span(step - 2 * per_role, CHUNK)], columns[...])

    @pl.when(step == 0)
    def _():
        input_out[...] = grad_in[...]
        conv_a[...] = sums[0, :taps, :]
        conv_v[...] = sums[1, :taps, :]
        bias_a[...] = sums[0, taps : taps + 1, :]
        bias_v[...] = sums[1, taps : taps + 1, :]
        rows_a[...] = norms[0:1, :]
        rows_v[...] = norms[1:2, :]
        rows_d[...] = down_norms[...]
        lane = lax.broadcasted_iota(jnp.int32, (1, 128), 1)
        for r in range(2):
            row = jnp.zeros((1, 128), F32)
            for k in range(taps):
                row = jnp.where(lane == k, squares[r, k : k + 1, :], row)
            conv_rows[r : r + 1, :] = row[:, :taps]


def weight_gradients(hidden_in, all_g, all_m, columns, sums, grad_in, norms, down_norms, squares):
    depth, width = hidden_in.shape[1], all_m.shape[1]
    taps = sums.shape[1] - 1
    per_role, per_down = depth // CHUNK, width // CHUNK
    operands = (hidden_in, all_g, all_m, columns, sums, grad_in, norms, down_norms, squares)

    def whole(shape):
        return pl.BlockSpec(shape, lambda i: (0,) * len(shape))

    small = (
        (grad_in.shape, BF16), ((taps, width), F32), ((taps, width), F32), ((1, width), F32),
        ((1, width), F32), ((1, depth), F32), ((1, depth), F32), ((1, width), F32),
        ((2, taps), F32),
    )
    return pl.pallas_call(
        weight_kernel,
        grid=(2 * per_role + per_down,),
        out_shape=(
            jax.ShapeDtypeStruct((depth, width), F32),
            jax.ShapeDtypeStruct((depth, width), F32),
            jax.ShapeDtypeStruct((width, depth), F32),
            *(jax.ShapeDtypeStruct(shape, dtype) for shape, dtype in small),
        ),
        in_specs=[whole(operand.shape) for operand in operands],
        out_specs=(
            pl.BlockSpec((CHUNK, width), lambda i: (jnp.minimum(i, per_role - 1), 0)),
            pl.BlockSpec(
                (CHUNK, width), lambda i: (jnp.clip(i - per_role, 0, per_role - 1), 0)
            ),
            pl.BlockSpec((CHUNK, depth), lambda i: (jnp.maximum(i - 2 * per_role, 0), 0)),
            *(whole(shape) for shape, _ in small),
        ),
        compiler_params=pltpu.CompilerParams(vmem_limit_bytes=40 * 1024 * 1024),
    )(*operands)


def with_kernels(
    hidden_in, up_act, up_val, cotangent, w_act, w_val, w_down,
    conv_act, conv_val, bias_act, bias_val,
):
    params = jnp.concatenate(
        [conv_act, bias_act[None, :], conv_val, bias_val[None, :]], 0
    ).astype(F32)
    columns, all_g, all_m, sums, grad_in, norms, down_norms, squares = gradients(
        hidden_in, up_act, up_val, cotangent, w_act, w_val, w_down, params
    )
    (
        grad_w_act, grad_w_val, grad_w_down, grad_input, conv_a, conv_v, bias_a, bias_v,
        rows_a, rows_v, rows_d, conv_rows,
    ) = weight_gradients(
        hidden_in, all_g, all_m, columns, sums, grad_in, norms, down_norms, squares
    )
    return (
        grad_input, grad_w_act, grad_w_val, grad_w_down, conv_a, conv_v,
        bias_a.reshape(-1), bias_v.reshape(-1), rows_a.reshape(-1), rows_v.reshape(-1),
        rows_d.reshape(-1), conv_rows,
    )


def passed_along(value, axis, by):
    length = lax.axis_size(axis)
    pairs = [(i, i + by) for i in range(length) if 0 <= i + by < length]
    return lax.ppermute(value, axis, pairs)


def contract_last(left, right):
    return lax.dot_general(
        left, right, (((1,), (1,)), ((), ())), preferred_element_type=jnp.float32
    )


def contract_first(left, right):
    return lax.dot_general(
        left, right, (((0,), (0,)), ((), ())), preferred_element_type=jnp.float32
    )


def conv_ahead(extended, taps, bias, length):
    total = jnp.zeros((length, extended.shape[1]), jnp.float32) + bias.astype(jnp.float32)
    for offset in range(taps.shape[0]):
        total = total + taps[offset].astype(jnp.float32) * extended[offset : offset + length]
    return total


def conv_behind(extended, taps, length):
    reach = taps.shape[0] - 1
    total = jnp.zeros((length, extended.shape[1]), jnp.float32)
    for offset in range(taps.shape[0]):
        total = (
            total
            + taps[offset].astype(jnp.float32) * extended[reach - offset : reach - offset + length]
        )
    return total.astype(jnp.bfloat16)


def tap_grads(grad_pre, extended, tap_count):
    length = grad_pre.shape[0]
    rows = [
        jnp.sum(grad_pre * extended[offset : offset + length], axis=0)
        for offset in range(tap_count)
    ]
    return (jnp.stack(rows, 0), jnp.sum(grad_pre, axis=0))


def per_device(
    hidden_in,
    up_act,
    up_val,
    cotangent,
    w_act,
    w_val,
    w_down,
    conv_act,
    conv_val,
    bias_act,
    bias_val,
):
    if kernels_fit(up_act, w_down, conv_act):
        return with_kernels(
            hidden_in, up_act, up_val, cotangent, w_act, w_val, w_down,
            conv_act, conv_val, bias_act, bias_val,
        )
    local_rows = cotangent.shape[0]
    tap_count = conv_act.shape[0]
    reach = tap_count - 1
    tp_count = lax.axis_size("tp")
    fs_count = lax.axis_size("fs")
    down_whole = lax.all_gather(w_down, "tp", axis=1, tiled=True)
    prev_act, prev_val = passed_along(
        (up_act[local_rows - reach :], up_val[local_rows - reach :]), "tp", 1
    )
    ext_act = jnp.concatenate([prev_act, up_act], 0).astype(jnp.float32)
    ext_val = jnp.concatenate([prev_val, up_val], 0).astype(jnp.float32)
    pre_act = conv_ahead(ext_act, conv_act, bias_act, local_rows)
    pre_val = conv_ahead(ext_val, conv_val, bias_val, local_rows)
    gelu_act, gelu_back = jax.vjp(jax.nn.gelu, pre_act)
    mixed = (gelu_act * pre_val).astype(jnp.bfloat16)
    grad_mixed = contract_last(cotangent, down_whole).astype(jnp.bfloat16)
    grad_mixed = lax.optimization_barrier(grad_mixed).astype(jnp.float32)
    grad_pre_act = gelu_back(grad_mixed * pre_val)[0]
    grad_pre_val = grad_mixed * gelu_act
    next_act, next_val = passed_along((grad_pre_act[:reach], grad_pre_val[:reach]), "tp", -1)
    grad_up_act = conv_behind(jnp.concatenate([grad_pre_act, next_act], 0), conv_act, local_rows)
    grad_up_val = conv_behind(jnp.concatenate([grad_pre_val, next_val], 0), conv_val, local_rows)
    taps_act, sums_act = tap_grads(grad_pre_act, ext_act, tap_count)
    taps_val, sums_val = tap_grads(grad_pre_val, ext_val, tap_count)
    all_up_act, all_up_val, all_mixed = (
        lax.all_gather(grad_up_act, "tp", axis=0, tiled=True),
        lax.all_gather(grad_up_val, "tp", axis=0, tiled=True),
        lax.all_gather(mixed, "tp", axis=0, tiled=True),
    )
    cot_columns = lax.all_to_all(cotangent, "tp", split_axis=1, concat_axis=0, tiled=True)
    grad_w_act = contract_first(hidden_in, all_up_act)
    grad_w_val = contract_first(hidden_in, all_up_val)
    grad_w_down = contract_first(all_mixed, cot_columns)
    shard_rows = local_rows // fs_count
    block_rows = tp_count * shard_rows

    def select_rows(gathered):
        shaped = gathered.reshape(tp_count, fs_count, shard_rows, gathered.shape[1])
        return jnp.transpose(shaped, (1, 0, 2, 3)).reshape(
            lax.axis_size("fs") * block_rows, gathered.shape[1]
        )

    summed = lax.psum_scatter(
        contract_last(select_rows(all_up_act), w_act)
        + contract_last(select_rows(all_up_val), w_val),
        "fs",
        scatter_dimension=0,
        tiled=True,
    ).astype(jnp.bfloat16)
    grad_input = lax.all_to_all(summed, "tp", split_axis=0, concat_axis=1, tiled=True)
    down_squares = jnp.sum(grad_w_down * grad_w_down, axis=1)
    taps_act, taps_val, sums_act, sums_val, rows_down = lax.psum(
        (taps_act, taps_val, sums_act, sums_val, down_squares), "tp"
    )
    tap_squares = jnp.stack(
        [jnp.sum(taps_act * taps_act, axis=1), jnp.sum(taps_val * taps_val, axis=1)], 0
    )
    rows_act, rows_val, conv_rows = lax.psum(
        (
            jnp.sum(grad_w_act * grad_w_act, axis=1),
            jnp.sum(grad_w_val * grad_w_val, axis=1),
            tap_squares,
        ),
        "fs",
    )
    return (
        grad_input,
        grad_w_act,
        grad_w_val,
        grad_w_down,
        taps_act,
        taps_val,
        sums_act,
        sums_val,
        rows_act,
        rows_val,
        rows_down,
        conv_rows,
    )


def solution(mesh):
    return jax.shard_map(
        per_device,
        mesh=mesh,
        in_specs=(
            P(None, "tp"),
            P("tp", "fs"),
            P("tp", "fs"),
            P("tp", None),
            P("tp", "fs"),
            P("tp", "fs"),
            P("fs", "tp"),
            P(None, "fs"),
            P(None, "fs"),
            P("fs"),
            P("fs"),
        ),
        out_specs=(
            P(("tp", "fs"), None),
            P("tp", "fs"),
            P("tp", "fs"),
            P("fs", "tp"),
            P(None, "fs"),
            P(None, "fs"),
            P("fs"),
            P("fs"),
            P("tp"),
            P("tp"),
            P("fs"),
            P(),
        ),
        check_vma=False,
    )
```

time: 127 us -> 109 us (0.86)
  Pallas kernels: 108 us -> 97.8 us
  local copies, waits for them, and re-layouts: 16.4 us -> 7.89 us
    pallas_call x4 -> x1, Pallas kernels: 43 us -> 12.9 us  [weight_gradients(): pl.pallas_call(weight_kernel, grid=(2 * per_role + per_down,), out_shape=...]
    pallas_call x1, Pallas kernels: 65.2 us -> 84.9 us  [gradients(): pl.pallas_call(gradient_kernel, out_shape=(jax.ShapeDtypeStruct((position...]
    slice x3 -> x0, local copies, waits for them, and re-layouts: 3.59 us -> none  [the longest x1 1.46 us: with_kernels(): sums[2 * tap_count + 1]]
    unnamed x23 -> x10, local copies, waits for them, and re-layouts: 9.99 us -> 6.5 us
    pallas_call x0 -> x3, other arithmetic: none -> 1.86 us  [weight_gradients(): pl.pallas_call(weight_kernel, grid=(2 * per_role + per_down,), out_shape=...]
    reshape x3 -> x0, local copies, waits for them, and re-layouts: 1.47 us -> none  [the longest x1 0.69 us: gradients(): bias_act.reshape(1, width)]
    broadcast_in_dim x1 -> x2, local copies, waits for them, and re-layouts: 0.01 us -> 1.38 us  [the longest x1 0.69 us: with_kernels(): bias_act[None, :]]
where the time goes in v1:
time: 109 us
  Pallas kernels  97.8 us (90%)
  local copies, waits for them, and re-layouts  7.89 us (7%)
  other arithmetic  2.61 us (2%)
    pallas_call x1, Pallas kernels, gradients(): pl.pallas_call(gradient_kernel, out_shape=(jax.ShapeDtypeStruct((position...  84.9 us
    pallas_call x1, Pallas kernels, weight_gradients(): pl.pallas_call(weight_kernel, grid=(2 * per_role + per_down,), out_shape=...  12.9 us
    unnamed x10, local copies, waits for them, and re-layouts  6.5 us

profile of v1, /device:TPU:0, one launch (start us, length us, event | category | flops | bytes accessed | tf_op | source)
XLA Modules:
  0.0 108.9 jit_solution(15337051915826722368)
XLA Ops:
  0.6 0.7 broadcast_in_dim.6
  1.3 0.7 broadcast_in_dim.7
  2.0 0.8 maximum_convert_fusion.params
  2.8 0.0 copy-start
  2.8 1.2 %copy-done = bf16[512,1024]{1,0:T(8,128)(2,1)S(1)} copy-done((bf16[512,1024]{1,0:T(8,128)(2,1)S(1)}, bf16[512,1024]{1,0:T(8,128)(2,1)}, u32[]{:S(2)}) %copy-start) | copy-done | bytes 1048600
  4.0 0.0 copy-start.3
  4.0 1.0 copy-done.3
  5.0 0.0 copy-start.4
  5.0 1.0 copy-done.4
  6.0 84.9 %shard_map.202 = (bf16[512,1024]{1,0:T(8,128)(2,1)S(1)}, bf16[2,512,1536]{2,1,0:T(8,128)(2,1)}, bf16[512,1536]{1,0:T(8,128)(2,1)}, f32[2,4,1536]{2,1,0:T(4,128)S...) custom-call(bf16[512,1024]{1,0:T(8,128)(2,1)S(1)} %copy-done, ...), custom_call_target="tpu_custom_call" | custom-call | tf_op jit(solution)/shard_map/pallas_call | solution.py:515
  90.9 0.0 copy-start.1
  90.9 1.9 %copy-done.1 = bf16[2,512,1536]{2,1,0:T(8,128)(2,1)S(1)} copy-done((bf16[2,512,1536]{2,1,0:T(8,128)(2,1)S(1)}, bf16[2,512,1536]{2,1,0:T(8,128)(2,1)}, u32[]{:S(2)}) %copy-start.1) | copy-done | bytes 3145752
  92.8 0.0 copy-start.2
  92.8 1.4 %copy-done.2 = bf16[512,1536]{1,0:T(8,128)(2,1)S(1)} copy-done((bf16[512,1536]{1,0:T(8,128)(2,1)S(1)}, bf16[512,1536]{1,0:T(8,128)(2,1)}, u32[]{:S(2)}) %copy-start.2) | copy-done | bytes 1572888
  94.2 12.9 %shard_map.203 = (f32[1024,1536]{1,0:T(8,128)}, f32[1024,1536]{1,0:T(8,128)}, f32[1536,1024]{1,0:T(8,128)}, bf16[16,4096]{1,0:T(8,128)(2,1)}, f32[3,1536]{1,0:T(...) custom-call(bf16[512,1024]{1,0:T(8,128)(2,1)S(1)} %copy-done, ...), custom_call_target="tpu_custom_call" | custom-call | tf_op jit(solution)/shard_map/pallas_call | solution.py:624
  107.1 0.6 reduce
  107.7 0.6 reduce.1
  108.3 0.6 reduce.2
Async XLA Ops:
  2.8 1.2 %copy-start = (bf16[512,1024]{1,0:T(8,128)(2,1)S(1)}, bf16[512,1024]{1,0:T(8,128)(2,1)}, u32[]{:S(2)}) copy-start(bf16[512,1024]{1,0:T(8,128)(2,1)} %hidden.1) | copy-start | bytes 3145732
  4.0 1.0 copy-start.3
  5.0 1.0 copy-start.4
  90.9 1.9 %copy-start.1 = (bf16[2,512,1536]{2,1,0:T(8,128)(2,1)S(1)}, bf16[2,512,1536]{2,1,0:T(8,128)(2,1)}, u32[]{:S(2)}) copy-start(bf16[2,512,1536]{2,1,0:T(8,128)(2,1)} %get-tuple-element.32.all_g) | copy-start | bytes 9437188
  92.8 1.4 %copy-start.2 = (bf16[512,1536]{1,0:T(8,128)(2,1)S(1)}, bf16[512,1536]{1,0:T(8,128)(2,1)}, u32[]{:S(2)}) copy-start(bf16[512,1536]{1,0:T(8,128)(2,1)} %get-tuple-element.33.all_m) | copy-start | bytes 4718596

commit v2 on v1

--- a/solution.py
+++ b/solution.py
@@ -15,6 +15,8 @@
 HALO = 16
 TAIL = 8
 COPIES = 112
+ROWS = 512
+SLOTS = 3
 ROOT_TWO_OVER_PI = 0.7978845608028654
 CUBIC = 0.044715
 
@@ -24,9 +26,10 @@
 
 
 def gradient_kernel(
-    hidden_hbm, up_a_hbm, up_v_hbm, cot_hbm, w_a_hbm, w_v_hbm, down_hbm, params,
+    hidden_hbm, up_a_hbm, up_v_hbm, cot_hbm, w_a_hbm, w_v_hbm, down_hbm,
+    taps_a_hbm, taps_v_hbm, bias_a_hbm, bias_v_hbm,
     columns, all_g, all_m, sums, out, norms, down_norms, squares,
-    hidden, up, cot, weights, down,
+    hidden, up, cot, weights, down, taps_a, taps_v, bias_a, bias_v, params,
     before, after, grads, gated, factor,
     own, to_sib, from_sib, to_sib_far, from_sib_far, to_far, from_far,
     terms, to_pair, from_pair, kept, to_line, from_line, settled,
@@ -45,7 +48,7 @@
     z_mate = z + 1 - 2 * (z % 2)
     length, width = up.shape[1:]
     depth = down.shape[1]
-    tap_count = params.shape[0] // 2 - 1
+    tap_count = taps_a.shape[0]
     reach = tap_count - 1
     group_count = width // GROUP
     shard = out.shape[0]
@@ -95,15 +98,18 @@
 
         lax.fori_loop(0, GROUP // CHUNK, at, 0)
 
-    def depth_chunks(step):
+    def depth_chunks(step, part=0, parts=1):
+        per_part = depth // (CHUNK * parts)
+
         def at(i, carry):
-            step(span(i, CHUNK))
+            step(span(part * per_part + i, CHUNK))
             return carry
 
-        lax.fori_loop(0, depth // CHUNK, at, 0)
+        lax.fori_loop(0, per_part, at, 0)
 
     sources = (
-        (up_a_hbm, up.at[0]), (up_v_hbm, up.at[1]), (cot_hbm, cot), (down_hbm, down),
+        (up_a_hbm, up.at[0]), (up_v_hbm, up.at[1]), (cot_hbm, cot), (taps_a_hbm, taps_a),
+        (taps_v_hbm, taps_v), (bias_a_hbm, bias_a), (bias_v_hbm, bias_v), (down_hbm, down),
         (hidden_hbm, hidden), (w_a_hbm, weights.at[0]), (w_v_hbm, weights.at[1]),
     )
     loads = [
@@ -139,14 +145,20 @@
         after[...] = jnp.zeros(after.shape, after.dtype)
 
     loads[2].wait()
+    for load in loads[3:7]:
+        load.wait()
+    for r, (taps, bias) in enumerate(((taps_a, bias_a), (taps_v, bias_v))):
+        at = r * (tap_count + 1)
+        params[at : at + tap_count, :] = taps[...].astype(F32)
+        params[at + tap_count : at + tap_count + 1, :] = bias[...].astype(F32)[None, :]
     mine = span((z % 2) * 2 + y, quarter)
 
     def quarter_of(index):
         at = index * length + ((z % 2) * 2 + y) * quarter
         return columns.at[pl.ds(pl.multiple_of(at, quarter), quarter), :]
 
+    cot_diag = launch(cot.at[mine, cols(diag)], quarter_of(me), to(diag))
     cot_far = launch(cot.at[mine, cols(far)], quarter_of(me), to(far))
-    cot_diag = launch(cot.at[mine, cols(diag)], quarter_of(me), to(diag))
     cot_sib = launch(cot.at[:, cols(sib)], columns.at[rows(me), :], to(sib))
     columns[rows(me), :] = cot[:, cols(me)]
 
@@ -194,18 +206,17 @@
         for copy in halo:
             copy.wait_recv()
 
-    shares = []
     for g in range(group_count):
         chunks(g, forward)
         spread_mixed(g)
         if g == 0:
+            cot_diag.wait_recv()
+            shared_diag = share(diag)
+        if g == 1:
             cot_far.wait_recv()
-            shares += share(far)
-        if g == 1:
-            cot_diag.wait_recv()
-            shares += share(diag)
-
-    loads[3].wait()
+            shared_far = share(far)
+
+    loads[7].wait()
 
     def partial(index, g, finish):
         def step(lanes):
@@ -228,9 +239,6 @@
     for g in range(group_count):
         partial(sib, g, keep(to_sib))
     near = launch(to_sib, from_sib, to(sib))
-    for copy in shares:
-        copy.wait_recv()
-
     relayed, crossed = [], []
 
     def diag_part(g):
@@ -242,9 +250,14 @@
         partial(far, g, add_far)
         crossed.append(launch(to_far.at[:, group(g)], from_far.at[:, group(g)], to(far)))
 
+    for copy in shared_diag:
+        copy.wait_recv()
     diag_part(0)
     for g in range(1, group_count):
         diag_part(g)
+        if g == 1:
+            for copy in shared_far:
+                copy.wait_recv()
         far_part(g - 1)
     far_part(group_count - 1)
 
@@ -277,7 +290,13 @@
 
     first = pl.ds(0, TAIL)
     left = lax.rem(me + count - 1, count)
-    backs, sent_g = [], []
+    final = group_count - 1
+    backs, sent_g = [], {}
+
+    def cross(g, j):
+        here = all_g.at[core, rows(chip * 2 + j), group(g)]
+        sent_g[g, j] = launch(here, here, to(far))
+
     near.wait_recv()
     for g in range(group_count):
         crossed[g].wait_recv()
@@ -309,14 +328,16 @@
             beside.append(launch(here, here, to(sib)))
         for copy in beside:
             copy.wait_recv()
-        for j in range(2):
-            here = all_g.at[core, rows(chip * 2 + j), group(g)]
-            sent_g.append(launch(here, here, to(far)))
+        cross(g, 0)
+        if g < final - 1:
+            cross(g, 1)
+    cross(final - 1, 1)
+    cross(final, 1)
     relay_mixed(group_count - 1)
     side_sums = launch(own_sums.at[1 - core], sib_sums, to(sib))
 
-    loads[5].wait()
-    loads[6].wait()
+    loads[9].wait()
+    loads[10].wait()
 
     def product(at, lanes, ks):
         total = contract_last(all_g[0, at, ks], weights[0, lanes, ks])
@@ -333,42 +354,50 @@
         return pl.ds(pl.multiple_of(blocks[k] * length + index * shard, shard), shard)
 
     pair_copies, line_copies, last_copies = {}, {}, {}
-
-    def send_pair(k):
+    parts = 2 if depth % (2 * CHUNK) == 0 else 1
+    whole = pl.ds(0, depth)
+
+    def part_of(part):
+        return pl.ds(part * (depth // parts), depth // parts)
+
+    def send_pair(k, part=None):
+        at = whole if part is None else part_of(part)
         for there in range(line):
-            to_pair[k, there * shard : (there + 1) * shard, :] = terms[
-                slab(k, there * 2 + (1 - y)), :
+            to_pair[k, there * shard : (there + 1) * shard, at] = terms[
+                slab(k, there * 2 + (1 - y)), at
             ].astype(BF16)
-        pair_copies[k] = launch(to_pair.at[k], from_pair.at[k], to_fs(pair))
-
-    def send_line(k):
-        pair_copies[k].wait_recv()
-        line_copies[k] = []
+        pair_copies[k, part] = launch(to_pair.at[k, :, at], from_pair.at[k, :, at], to_fs(pair))
+
+    def send_line(k, part=None):
+        at = whole if part is None else part_of(part)
+        pair_copies[k, part].wait_recv()
+        line_copies[k, part] = []
         for by in sorted(range(1, line), key=lambda by: -min(by, line - by)) + [0]:
             there = lax.rem(z + by, line)
-            added = terms[slab(k, there * 2 + y), :] + from_pair[
-                k, span(there, shard), :
+            added = terms[slab(k, there * 2 + y), at] + from_pair[
+                k, span(there, shard), at
             ].astype(F32)
             if by == 0:
-                kept[k] = added
+                kept[k, :, at] = added
             else:
-                to_line[k, by] = added.astype(BF16)
-                line_copies[k].append(
-                    (by, launch(to_line.at[k, by], from_line.at[k, by], to_fs(there * 2 + y)))
-                )
+                to_line[k, by, :, at] = added.astype(BF16)
+                line_copies[k, part].append((by, launch(
+                    to_line.at[k, by, :, at], from_line.at[k, by, :, at], to_fs(there * 2 + y)
+                )))
 
     a2a = [next(numbers) for _ in range(2)]
 
-    def settle(k):
-        total = kept[k]
-        for by, copy in line_copies[k]:
-            copy.wait_recv()
-            total = total + from_line[k, by].astype(F32)
+    def settle(k, split=(None,)):
+        for part in split:
+            at = whole if part is None else part_of(part)
+            total = kept[k, :, at]
+            for by, copy in line_copies[k, part]:
+                copy.wait_recv()
+                total = total + from_line[k, by, :, at].astype(F32)
+            settled[k, :, at] = total.astype(BF16)
         if k == 0:
-            out[:, cols(me)] = total.astype(BF16)
-            return
-        settled[k] = total.astype(BF16)
-        if k == 1:
+            out[:, cols(me)] = settled[k]
+        elif k == 1:
             last_copies[k] = launch(settled.at[k], out.at[:, cols(me)], to(sib))
         else:
             last_copies[k] = copy_of(
@@ -385,7 +414,7 @@
         copy.wait_recv()
     for copy in mixed_relays:
         copy.wait_recv()
-    loads[4].wait()
+    loads[8].wait()
     own_down[...] = jnp.zeros(own_down.shape, F32)
 
     def down_step(lanes):
@@ -416,28 +445,35 @@
     theirs = span(other, 2 * length)
 
     def relay_g(g, j):
-        sent_g[2 * g + j].wait_recv()
+        sent_g[g, j].wait_recv()
         there = all_g.at[core, rows(other * 2 + j), group(g)]
         return launch(there, there, to(sib))
 
-    for g in range(group_count - 1):
-        relays = [relay_g(g, j) for j in range(2)]
-        for copy in relays:
+    def take(*which):
+        for copy in [relay_g(g, j) for g, j in which]:
             copy.wait_recv()
 
-        def add_group(lanes):
-            value = product(theirs, lanes, group(g))
-            terms[theirs, lanes] = value if g == 0 else terms[theirs, lanes] + value
-
-        depth_chunks(add_group)
+    def add(at, ks, fresh, part=0, split=1):
+        def step(lanes):
+            value = product(at, lanes, ks)
+            terms[at, lanes] = value if fresh else terms[at, lanes] + value
+
+        depth_chunks(step, part, split)
+
+    for g in range(final - 1):
+        take((g, 0), (g, 1))
+        add(theirs, group(g), g == 0)
         if g == 0:
             cross_sums.wait_recv()
             sums[core] = chip_sums[...] + far_sums[...]
             side_total = launch(sums.at[core], sums.at[core], to(sib))
             settle(0)
             settle(1)
+    for g in range(final - 1):
         norm_group(g)
-
+    take((final - 1, 0), (final, 0))
+    add(rows(other * 2), pl.ds((final - 1) * GROUP, 2 * GROUP), final == 1)
+    send_pair(2)
     side_total.wait_recv()
     total_sums = sums[...]
     own_squares[...] = jnp.broadcast_to(
@@ -445,25 +481,21 @@
     )
     got_squares[fs] = own_squares[...]
     square_copies = [launch(own_squares, got_squares.at[fs], to_fs(index)) for index in fs_others]
-
-    g = group_count - 1
-    for j in range(2):
-        relay_g(g, j).wait_recv()
-        at = rows(other * 2 + j)
-
-        def add_last(lanes):
-            value = product(at, lanes, group(g))
-            terms[at, lanes] = value if g == 0 else terms[at, lanes] + value
-
-        depth_chunks(add_last)
-        send_pair(2 + j)
-    norm_group(g)
+    take((final - 1, 1))
+    add(rows(other * 2 + 1), group(final - 1), final == 1)
+    send_line(2)
+    norm_group(final - 1)
+    take((final, 1))
+    for part in range(parts):
+        add(rows(other * 2 + 1), group(final), False, part, parts)
+        send_pair(3, part)
+    norm_group(final)
     got_norms[fs] = own_norms[...]
     norm_copies = [launch(own_norms, got_norms.at[fs], to_fs(index)) for index in fs_others]
-    send_line(2)
-    send_line(3)
+    for part in range(parts):
+        send_line(3, part)
     settle(2)
-    settle(3)
+    settle(3, range(parts))
     for copies in (down_copies, square_copies, norm_copies):
         for copy in copies:
             copy.wait_recv()
@@ -497,16 +529,19 @@
             copy.wait_send()
 
 
-def gradients(hidden_in, up_act, up_val, cotangent, w_act, w_val, w_down, params):
+def gradients(
+    hidden_in, up_act, up_val, cotangent, w_act, w_val, w_down,
+    conv_act, conv_val, bias_act, bias_val,
+):
     length, width = up_act.shape
     depth = w_down.shape[1]
     tp_count, fs_count = lax.axis_size("tp"), lax.axis_size("fs")
     positions = length * tp_count
     shard = length // fs_count
     line = fs_count // 2
-    stat_rows = params.shape[0] // 2
+    stat_rows = conv_act.shape[0] + 1
     vmem = pl.BlockSpec(memory_space=pltpu.VMEM)
-    hbm = pl.BlockSpec(memory_space=pl.ANY)
+    hbm = pl.BlockSpec(memory_space=pltpu.HBM)
     block = pltpu.VMEM((length, width), BF16)
     wide = pltpu.VMEM((length, width), F32)
     slots = pltpu.VMEM((4, line * shard, depth), BF16)
@@ -524,7 +559,7 @@
             jax.ShapeDtypeStruct((1, width), F32),
             jax.ShapeDtypeStruct((2, stat_rows, 128), F32),
         ),
-        in_specs=[hbm] * 7 + [vmem],
+        in_specs=[hbm] * 11,
         out_specs=(vmem,) * 8,
         scratch_shapes=[
             pltpu.VMEM(hidden_in.shape, BF16),
@@ -532,6 +567,9 @@
             pltpu.VMEM(cotangent.shape, BF16),
             pltpu.VMEM((2,) + w_act.shape, BF16),
             pltpu.VMEM(w_down.shape, BF16),
+            pltpu.VMEM(conv_act.shape, BF16), pltpu.VMEM(conv_val.shape, BF16),
+            pltpu.VMEM((width,), BF16), pltpu.VMEM((width,), BF16),
+            pltpu.VMEM((2 * stat_rows, width), F32),
             pltpu.VMEM((2, HALO, width), BF16), pltpu.VMEM((2, TAIL, width), F32),
             pltpu.VMEM((2, length, width), F32), wide, wide,
             wide, block, block, block, block, block, block,
@@ -543,12 +581,18 @@
             pltpu.VMEM((1, width), F32), pltpu.VMEM((tp_count, 1, width), F32),
             pltpu.VMEM((2, stat_rows, 128), F32), pltpu.VMEM((fs_count, 2, stat_rows, 128), F32),
             pltpu.SemaphoreType.DMA((COPIES,)), pltpu.SemaphoreType.DMA((COPIES,)),
-            pltpu.SemaphoreType.DMA((7,)),
+            pltpu.SemaphoreType.DMA((11,)),
         ],
         compiler_params=pltpu.CompilerParams(
-            collective_id=0, has_side_effects=True, vmem_limit_bytes=50 * 1024 * 1024
+            collective_id=0, has_side_effects=True, vmem_limit_bytes=34 * 1024 * 1024
         ),
-    )(hidden_in, up_act, up_val, cotangent, w_act, w_val, w_down, params)
+    )(*(
+        pltpu.with_memory_space_constraint(operand, pltpu.HBM)
+        for operand in (
+            hidden_in, up_act, up_val, cotangent, w_act, w_val, w_down,
+            conv_act, conv_val, bias_act, bias_val,
+        )
+    ))
 
 
 def kernels_fit(up_act, w_down, conv_act):
@@ -558,8 +602,9 @@
         tp_count == 4
         and fs_count % 4 == 0
         and width % GROUP == 0
-        and width // GROUP > 1
-        and w_down.shape[1] % CHUNK == 0
+        and width // GROUP > 2
+        and w_down.shape[1] % ROWS == 0
+        and width % ROWS == 0
         and length % (16 * fs_count) == 0
         and conv_act.shape[0] - 1 <= TAIL
         and conv_act.shape[0] == 3
@@ -571,75 +616,78 @@
     hidden, all_g, all_m, columns, sums, grad_in, norms, down_norms, squares,
     w_act, w_val, w_down, input_out, conv_a, conv_v, bias_a, bias_v,
     rows_a, rows_v, rows_d, conv_rows,
+    blocks, held_conv, held_rows, held_a, held_v, held_d, held_rows_a, held_rows_v,
+    done, small_done,
 ):
-    step = pl.program_id(0)
-    per_role = pl.num_programs(0) - all_m.shape[1] // CHUNK
-    per_role = per_role // 2
     taps = conv_a.shape[0]
-
-    @pl.when(step < per_role)
-    def _():
-        w_act[...] = contract_first(hidden[:, span(step, CHUNK)], all_g[0])
-
-    @pl.when(jnp.logical_and(step >= per_role, step < 2 * per_role))
-    def _():
-        w_val[...] = contract_first(hidden[:, span(step - per_role, CHUNK)], all_g[1])
-
-    @pl.when(step >= 2 * per_role)
-    def _():
-        w_down[...] = contract_first(all_m[:, span(step - 2 * per_role, CHUNK)], columns[...])
-
-    @pl.when(step == 0)
-    def _():
-        input_out[...] = grad_in[...]
-        conv_a[...] = sums[0, :taps, :]
-        conv_v[...] = sums[1, :taps, :]
-        bias_a[...] = sums[0, taps : taps + 1, :]
-        bias_v[...] = sums[1, taps : taps + 1, :]
-        rows_a[...] = norms[0:1, :]
-        rows_v[...] = norms[1:2, :]
-        rows_d[...] = down_norms[...]
-        lane = lax.broadcasted_iota(jnp.int32, (1, 128), 1)
-        for r in range(2):
-            row = jnp.zeros((1, 128), F32)
-            for k in range(taps):
-                row = jnp.where(lane == k, squares[r, k : k + 1, :], row)
-            conv_rows[r : r + 1, :] = row[:, :taps]
+    depth, width = hidden.shape[1], all_m.shape[1]
+    for r in range(2):
+        held_conv[r] = sums[r, :taps, :]
+    held_a[...] = sums[0, taps, :]
+    held_v[...] = sums[1, taps, :]
+    held_d[...] = down_norms[0, :]
+    held_rows_a[...] = norms[0, :]
+    held_rows_v[...] = norms[1, :]
+    lane = lax.broadcasted_iota(jnp.int32, (1, 128), 1)
+    for r in range(2):
+        row = jnp.zeros((1, 128), F32)
+        for k in range(taps):
+            row = jnp.where(lane == k, squares[r, k : k + 1, :], row)
+        held_rows[r : r + 1, :] = row[:, :taps]
+    pairs = (
+        (grad_in, input_out), (held_conv.at[0], conv_a), (held_conv.at[1], conv_v),
+        (held_a, bias_a), (held_v, bias_v), (held_rows_a, rows_a),
+        (held_rows_v, rows_v), (held_d, rows_d), (held_rows, conv_rows),
+    )
+    flying = [
+        pltpu.make_async_copy(source, target, small_done.at[i])
+        for i, (source, target) in enumerate(pairs)
+    ]
+    for copy in flying:
+        copy.start()
+    jobs = [(hidden, all_g.at[0], w_act, at) for at in range(0, depth, ROWS)]
+    jobs += [(hidden, all_g.at[1], w_val, at) for at in range(0, depth, ROWS)]
+    jobs += [(all_m, columns, w_down, at) for at in range(0, width, ROWS)]
+    stored = []
+    for number, (left, right, target, at) in enumerate(jobs):
+        slot = number % SLOTS
+        if number >= SLOTS:
+            stored[number - SLOTS].wait()
+        size = right.shape[1]
+        blocks[slot, :, :size] = contract_first(left[:, at : at + ROWS], right[...])
+        stored.append(pltpu.make_async_copy(
+            blocks.at[slot, :, pl.ds(0, size)], target.at[pl.ds(at, ROWS), :], done.at[slot]
+        ))
+        stored[number].start()
+    for copy in stored[-SLOTS:] + flying:
+        copy.wait()
 
 
 def weight_gradients(hidden_in, all_g, all_m, columns, sums, grad_in, norms, down_norms, squares):
     depth, width = hidden_in.shape[1], all_m.shape[1]
     taps = sums.shape[1] - 1
-    per_role, per_down = depth // CHUNK, width // CHUNK
     operands = (hidden_in, all_g, all_m, columns, sums, grad_in, norms, down_norms, squares)
-
-    def whole(shape):
-        return pl.BlockSpec(shape, lambda i: (0,) * len(shape))
-
-    small = (
-        (grad_in.shape, BF16), ((taps, width), F32), ((taps, width), F32), ((1, width), F32),
-        ((1, width), F32), ((1, depth), F32), ((1, depth), F32), ((1, width), F32),
-        ((2, taps), F32),
+    shapes = (
+        (depth, width), (depth, width), (width, depth), None, (taps, width), (taps, width),
+        (width,), (width,), (depth,), (depth,), (width,), (2, taps),
     )
     return pl.pallas_call(
         weight_kernel,
-        grid=(2 * per_role + per_down,),
-        out_shape=(
-            jax.ShapeDtypeStruct((depth, width), F32),
-            jax.ShapeDtypeStruct((depth, width), F32),
-            jax.ShapeDtypeStruct((width, depth), F32),
-            *(jax.ShapeDtypeStruct(shape, dtype) for shape, dtype in small),
+        out_shape=tuple(
+            jax.ShapeDtypeStruct(grad_in.shape, BF16) if shape is None
+            else jax.ShapeDtypeStruct(shape, F32)
+            for shape in shapes
         ),
-        in_specs=[whole(operand.shape) for operand in operands],
-        out_specs=(
-            pl.BlockSpec((CHUNK, width), lambda i: (jnp.minimum(i, per_role - 1), 0)),
-            pl.BlockSpec(
-                (CHUNK, width), lambda i: (jnp.clip(i - per_role, 0, per_role - 1), 0)
-            ),
-            pl.BlockSpec((CHUNK, depth), lambda i: (jnp.maximum(i - 2 * per_role, 0), 0)),
-            *(whole(shape) for shape, _ in small),
-        ),
-        compiler_params=pltpu.CompilerParams(vmem_limit_bytes=40 * 1024 * 1024),
+        in_specs=[pl.BlockSpec(memory_space=pltpu.VMEM)] * len(operands),
+        out_specs=(pl.BlockSpec(memory_space=pltpu.HBM),) * len(shapes),
+        scratch_shapes=[
+            pltpu.VMEM((SLOTS, ROWS, max(depth, width)), F32),
+            pltpu.VMEM((2, taps, width), F32), pltpu.VMEM((2, taps), F32),
+            pltpu.VMEM((width,), F32), pltpu.VMEM((width,), F32), pltpu.VMEM((width,), F32),
+            pltpu.VMEM((depth,), F32), pltpu.VMEM((depth,), F32),
+            pltpu.SemaphoreType.DMA((SLOTS,)), pltpu.SemaphoreType.DMA((9,)),
+        ],
+        compiler_params=pltpu.CompilerParams(vmem_limit_bytes=24 * 1024 * 1024),
     )(*operands)
 
 
@@ -647,11 +695,9 @@
     hidden_in, up_act, up_val, cotangent, w_act, w_val, w_down,
     conv_act, conv_val, bias_act, bias_val,
 ):
-    params = jnp.concatenate(
-        [conv_act, bias_act[None, :], conv_val, bias_val[None, :]], 0
-    ).astype(F32)
     columns, all_g, all_m, sums, grad_in, norms, down_norms, squares = gradients(
-        hidden_in, up_act, up_val, cotangent, w_act, w_val, w_down, params
+        hidden_in, up_act, up_val, cotangent, w_act, w_val, w_down,
+        conv_act, conv_val, bias_act, bias_val,
     )
     (
         grad_w_act, grad_w_val, grad_w_down, grad_input, conv_a, conv_v, bias_a, bias_v,
@@ -661,8 +707,7 @@
     )
     return (
         grad_input, grad_w_act, grad_w_val, grad_w_down, conv_a, conv_v,
-        bias_a.reshape(-1), bias_v.reshape(-1), rows_a.reshape(-1), rows_v.reshape(-1),
-        rows_d.reshape(-1), conv_rows,
+        bias_a, bias_v, rows_a, rows_v, rows_d, conv_rows,
     )
 
 

time: 109 us -> 87.8 us (0.81)
  Pallas kernels: 97.8 us -> 87 us
  local copies, waits for them, and re-layouts: 7.89 us -> 0.01 us
  other arithmetic: 2.61 us -> 0 us
    unnamed x10 -> x2, local copies, waits for them, and re-layouts: 6.5 us -> 0.01 us
    pallas_call x1, Pallas kernels: 84.9 us -> 79 us  [gradients(): pl.pallas_call(gradient_kernel, out_shape=(jax.ShapeDtypeStruct((position...]
    pallas_call x1, Pallas kernels: 12.9 us -> 7.94 us  [weight_gradients(): pl.pallas_call(weight_kernel, out_shape=tuple((jax.ShapeDtypeStruct(grad_...]
    pallas_call x3 -> x0, other arithmetic: 1.86 us -> none  [weight_gradients(): pl.pallas_call(weight_kernel, grid=(2 * per_role + per_down,), out_shape=...]
    broadcast_in_dim x2 -> x0, local copies, waits for them, and re-layouts: 1.38 us -> none  [the longest x1 0.69 us: with_kernels(): bias_act[None, :]]
where the time goes in v2:
time: 87.8 us; the launch traced here: 87.6 us
  Pallas kernels  87 us (99%)
    pallas_call x1, Pallas kernels, gradients(): pl.pallas_call(gradient_kernel, out_shape=(jax.ShapeDtypeStruct((position...  79 us
    pallas_call x1, Pallas kernels, weight_gradients(): pl.pallas_call(weight_kernel, out_shape=tuple((jax.ShapeDtypeStruct(grad_...  7.94 us

profile of v2, /device:TPU:0, one launch (start us, length us, event | category | flops | bytes accessed | tf_op | source)
XLA Modules:
  0.0 87.6 jit_solution(13878070198600260023)
XLA Ops:
  0.6 0.0 copy-start
  0.7 79.0 %shard_map.202 = (bf16[512,1024]{1,0:T(8,128)(2,1)S(1)}, bf16[2,512,1536]{2,1,0:T(8,128)(2,1)S(1)}, bf16[512,1536]{1,0:T(8,128)(2,1)S(1)}, f32[2,4,1536]{2,1,0:T...) custom-call(bf16[512,1024]{1,0:T(8,128)(2,1)} %hidden.1, ...), custom_call_target="tpu_custom_call" | custom-call | tf_op jit(solution)/shard_map/pallas_call | solution.py:550
  79.7 0.0 copy-done
  79.7 7.9 %shard_map.203 = (f32[1024,1536]{1,0:T(8,128)}, f32[1024,1536]{1,0:T(8,128)}, f32[1536,1024]{1,0:T(8,128)}, bf16[16,4096]{1,0:T(8,128)(2,1)}, f32[3,1536]{1,0:T(...) custom-call(bf16[512,1024]{1,0:T(8,128)(2,1)S(1)} %copy-done, ...), custom_call_target="tpu_custom_call" | custom-call | tf_op jit(solution)/shard_map/pallas_call | solution.py:674
Async XLA Ops:
  0.6 79.0 %copy-start = (bf16[512,1024]{1,0:T(8,128)(2,1)S(1)}, bf16[512,1024]{1,0:T(8,128)(2,1)}, u32[]{:S(2)}) copy-start(bf16[512,1024]{1,0:T(8,128)(2,1)} %hidden.1) | copy-start | bytes 3145732

commit v3 on v2

--- a/solution.py
+++ b/solution.py
@@ -12,9 +12,9 @@
 BF16 = jnp.bfloat16
 CHUNK = 256
 GROUP = 512
-HALO = 16
+HALO = 8
 TAIL = 8
-COPIES = 112
+COPIES = 144
 ROWS = 512
 SLOTS = 3
 ROOT_TWO_OVER_PI = 0.7978845608028654
@@ -32,7 +32,7 @@
     hidden, up, cot, weights, down, taps_a, taps_v, bias_a, bias_v, params,
     before, after, grads, gated, factor,
     own, to_sib, from_sib, to_sib_far, from_sib_far, to_far, from_far,
-    terms, to_pair, from_pair, kept, to_line, from_line, settled,
+    terms, to_pair, from_pair, kept, to_line, from_line, settled, arrived,
     own_sums, sib_sums, chip_sums, far_sums, own_norms, got_norms, own_down, got_down,
     own_squares, got_squares,
     send, receive, loaded,
@@ -116,11 +116,14 @@
         pltpu.make_async_copy(source, target, loaded.at[i])
         for i, (source, target) in enumerate(sources)
     ]
-    for load in loads:
+    for load in loads[:7]:
         load.start()
 
+    after[...] = jnp.zeros(after.shape, after.dtype)
     barrier = pltpu.get_barrier_semaphore()
+    z_others = [lax.rem(z + by, line) * 2 + y for by in range(1, line)]
     everyone = [to(sib), to(far), to(diag)] + [to_fs(index) for index in fs_others]
+    everyone += [{"tp": there, "fs": index} for index in z_others for there in (far, diag)]
     for where in everyone:
         pl.semaphore_signal(barrier, inc=1, device_id=where, device_id_type=MESH)
     pl.semaphore_wait(barrier, len(everyone))
@@ -139,10 +142,6 @@
     @pl.when(jnp.logical_not(has_before))
     def _():
         before[...] = jnp.zeros(before.shape, before.dtype)
-
-    @pl.when(jnp.logical_not(has_after))
-    def _():
-        after[...] = jnp.zeros(after.shape, after.dtype)
 
     loads[2].wait()
     for load in loads[3:7]:
@@ -160,6 +159,8 @@
     cot_diag = launch(cot.at[mine, cols(diag)], quarter_of(me), to(diag))
     cot_far = launch(cot.at[mine, cols(far)], quarter_of(me), to(far))
     cot_sib = launch(cot.at[:, cols(sib)], columns.at[rows(me), :], to(sib))
+    for load in loads[7:]:
+        load.start()
     columns[rows(me), :] = cot[:, cols(me)]
 
     def share(index):
@@ -268,6 +269,21 @@
         there = all_m.at[rows(far), group(g)]
         mixed_relays.append(launch(there, there, to(sib)))
 
+    for g in range(group_count):
+        relay_mixed(g)
+    for copy in mixed_sib + mixed_relays:
+        copy.wait_recv()
+    own_down[...] = jnp.zeros(own_down.shape, F32)
+
+    def down_step(lanes):
+        value = contract_first(columns[:, lanes], all_m[...])
+        own_down[...] += jnp.sum(value * value, axis=0, keepdims=True)
+
+    depth_chunks(down_step)
+    got_down[me] = own_down[...]
+    tp_others = [lax.rem(me + by, count) for by in range(1, count)]
+    down_copies = [launch(own_down, got_down.at[me], to(index)) for index in tp_others]
+
     def combine(lanes):
         total = own[:, lanes] + from_sib[:, lanes].astype(F32) + from_far[:, lanes].astype(F32)
         grad_mixed = total.astype(BF16).astype(F32)
@@ -288,7 +304,7 @@
                 total = total + param(r, k, lanes) * ext[reach - k : reach - k + length]
             all_g[r, rows(me), lanes] = total.astype(BF16)
 
-    first = pl.ds(0, TAIL)
+    first = pl.ds(0, reach)
     left = lax.rem(me + count - 1, count)
     final = group_count - 1
     backs, sent_g = [], {}
@@ -302,7 +318,7 @@
         crossed[g].wait_recv()
         chunks(g, combine)
         back = [
-            copy_of(grads.at[r, first, group(g)], after.at[r, :, group(g)], to(left))
+            copy_of(grads.at[r, first, group(g)], after.at[r, first, group(g)], to(left))
             for r in range(2)
         ]
         backs += back
@@ -311,10 +327,6 @@
         def _():
             for copy in back:
                 copy.start()
-
-        if g == 0:
-            for early in range(group_count - 1):
-                relay_mixed(early)
 
         @pl.when(has_after)
         def _():
@@ -333,7 +345,6 @@
             cross(g, 1)
     cross(final - 1, 1)
     cross(final, 1)
-    relay_mixed(group_count - 1)
     side_sums = launch(own_sums.at[1 - core], sib_sums, to(sib))
 
     loads[9].wait()
@@ -344,10 +355,6 @@
         return total + contract_last(all_g[1, at, ks], weights[1, lanes, ks])
 
     both = span(chip, 2 * length)
-    depth_chunks(lambda lanes: terms.__setitem__(
-        (both, lanes), product(both, lanes, pl.ds(0, width))
-    ))
-
     blocks = (me, sib, other * 2, other * 2 + 1)
 
     def slab(k, index):
@@ -367,6 +374,8 @@
                 slab(k, there * 2 + (1 - y)), at
             ].astype(BF16)
         pair_copies[k, part] = launch(to_pair.at[k, :, at], from_pair.at[k, :, at], to_fs(pair))
+
+    straight = {by: [next(numbers) for _ in range(2)] for by in range(line)}
 
     def send_line(k, part=None):
         at = whole if part is None else part_of(part)
@@ -377,7 +386,16 @@
             added = terms[slab(k, there * 2 + y), at] + from_pair[
                 k, span(there, shard), at
             ].astype(F32)
-            if by == 0:
+            if k >= 2:
+                to_line[k, by, :, at] = added.astype(BF16)
+                copy = copy_of(
+                    to_line.at[k, by, :, at], arrived.at[core, by, :, at],
+                    {"tp": blocks[k], "fs": there * 2 + y},
+                    receive_at=straight[by][0] + core,
+                )
+                copy.start()
+                pending.append(copy)
+            elif by == 0:
                 kept[k, :, at] = added
             else:
                 to_line[k, by, :, at] = added.astype(BF16)
@@ -385,95 +403,85 @@
                     to_line.at[k, by, :, at], from_line.at[k, by, :, at], to_fs(there * 2 + y)
                 )))
 
-    a2a = [next(numbers) for _ in range(2)]
-
-    def settle(k, split=(None,)):
-        for part in split:
-            at = whole if part is None else part_of(part)
-            total = kept[k, :, at]
-            for by, copy in line_copies[k, part]:
-                copy.wait_recv()
-                total = total + from_line[k, by, :, at].astype(F32)
-            settled[k, :, at] = total.astype(BF16)
+    def settle(k):
+        total = kept[k]
+        for by, copy in line_copies[k, None]:
+            copy.wait_recv()
+            total = total + from_line[k, by].astype(F32)
         if k == 0:
-            out[:, cols(me)] = settled[k]
-        elif k == 1:
-            last_copies[k] = launch(settled.at[k], out.at[:, cols(me)], to(sib))
+            out[:, cols(me)] = total.astype(BF16)
         else:
-            last_copies[k] = copy_of(
-                settled.at[k], out.at[:, cols(me)], to(blocks[k]),
-                send_at=a2a[k - 2], receive_at=a2a[0] + core,
-            )
-            last_copies[k].start()
-            pending.append(last_copies[k])
-
+            settled[...] = total.astype(BF16)
+            last_copies[k] = launch(settled, out.at[:, cols(me)], to(sib))
+
+    def settle_straight():
+        for j in range(2):
+            total = None
+            for by in range(line):
+                copy_of(
+                    arrived.at[j, by], arrived.at[j, by], to(far), receive_at=straight[by][j]
+                ).wait_recv()
+                value = arrived[j, by].astype(F32)
+                total = value if total is None else total + value
+            out[:, cols(other * 2 + j)] = total.astype(BF16)
+
+    def relay(*which):
+        started = []
+        for g, j in which:
+            sent_g[g, j].wait_recv()
+            there = all_g.at[core, rows(other * 2 + j), group(g)]
+            started.append(launch(there, there, to(sib)))
+        return started
+
+    def arrive(started):
+        for copy in started:
+            copy.wait_recv()
+
+    def add(at, g, fresh=False, part=0, split=1):
+        def step(lanes):
+            value = product(at, lanes, group(g))
+            terms[at, lanes] = value if fresh else terms[at, lanes] + value
+
+        depth_chunks(step, part, split)
+
+    own_norms[...] = jnp.zeros(own_norms.shape, F32)
+
+    def norm_group(g, roles=(0, 1)):
+        def step(lanes):
+            for r in roles:
+                value = contract_first(all_g[r, :, lanes], hidden[...])
+                own_norms[r : r + 1, :] += jnp.sum(value * value, axis=0, keepdims=True)
+
+        chunks(g, step)
+
+    theirs = span(other, 2 * length)
+    near_block, last_block = rows(other * 2), rows(other * 2 + 1)
+    started = relay((0, 0))
+    depth_chunks(lambda lanes: terms.__setitem__(
+        (both, lanes), product(both, lanes, pl.ds(0, width))
+    ))
     send_pair(0)
     send_pair(1)
-
-    for copy in mixed_sib:
-        copy.wait_recv()
-    for copy in mixed_relays:
-        copy.wait_recv()
-    loads[8].wait()
-    own_down[...] = jnp.zeros(own_down.shape, F32)
-
-    def down_step(lanes):
-        value = contract_first(columns[:, lanes], all_m[...])
-        own_down[...] += jnp.sum(value * value, axis=0, keepdims=True)
-
-    depth_chunks(down_step)
-    got_down[me] = own_down[...]
-    tp_others = [lax.rem(me + by, count) for by in range(1, count)]
-    down_copies = [launch(own_down, got_down.at[me], to(index)) for index in tp_others]
-
+    started += relay((0, 1))
     side_sums.wait_recv()
     chip_sums[...] = own_sums[core] + sib_sums[...]
     cross_sums = launch(chip_sums, far_sums, to(far))
+    loads[8].wait()
+    for g in range(final - 1):
+        if g > 0:
+            started = relay((g, 0), (g, 1))
+        arrive(started)
+        add(theirs, g, g == 0)
+        norm_group(g)
+    started = relay((final - 1, 0))
+    cross_sums.wait_recv()
+    sums[core] = chip_sums[...] + far_sums[...]
+    side_total = launch(sums.at[core], sums.at[core], to(sib))
     send_line(0)
     send_line(1)
-
-    own_norms[...] = jnp.zeros(own_norms.shape, F32)
-
-    def norm_group(g):
-        def step(lanes):
-            for r in range(2):
-                value = contract_first(all_g[r, :, lanes], hidden[...])
-                own_norms[r : r + 1, :] += jnp.sum(value * value, axis=0, keepdims=True)
-
-        chunks(g, step)
-
-    theirs = span(other, 2 * length)
-
-    def relay_g(g, j):
-        sent_g[g, j].wait_recv()
-        there = all_g.at[core, rows(other * 2 + j), group(g)]
-        return launch(there, there, to(sib))
-
-    def take(*which):
-        for copy in [relay_g(g, j) for g, j in which]:
-            copy.wait_recv()
-
-    def add(at, ks, fresh, part=0, split=1):
-        def step(lanes):
-            value = product(at, lanes, ks)
-            terms[at, lanes] = value if fresh else terms[at, lanes] + value
-
-        depth_chunks(step, part, split)
-
-    for g in range(final - 1):
-        take((g, 0), (g, 1))
-        add(theirs, group(g), g == 0)
-        if g == 0:
-            cross_sums.wait_recv()
-            sums[core] = chip_sums[...] + far_sums[...]
-            side_total = launch(sums.at[core], sums.at[core], to(sib))
-            settle(0)
-            settle(1)
-    for g in range(final - 1):
-        norm_group(g)
-    take((final - 1, 0), (final, 0))
-    add(rows(other * 2), pl.ds((final - 1) * GROUP, 2 * GROUP), final == 1)
-    send_pair(2)
+    arrive(started)
+    add(near_block, final - 1)
+    started = relay((final, 0))
     side_total.wait_recv()
     total_sums = sums[...]
     own_squares[...] = jnp.broadcast_to(
@@ -481,21 +489,26 @@
     )
     got_squares[fs] = own_squares[...]
     square_copies = [launch(own_squares, got_squares.at[fs], to_fs(index)) for index in fs_others]
-    take((final - 1, 1))
-    add(rows(other * 2 + 1), group(final - 1), final == 1)
+    arrive(started)
+    add(near_block, final)
+    send_pair(2)
+    arrive(relay((final - 1, 1)))
+    add(last_block, final - 1)
+    norm_group(final - 1, (0,))
+    started = relay((final, 1))
+    norm_group(final - 1, (1,))
+    arrive(started)
+    for part in range(parts):
+        add(last_block, final, False, part, parts)
+        send_pair(3, part)
     send_line(2)
-    norm_group(final - 1)
-    take((final, 1))
-    for part in range(parts):
-        add(rows(other * 2 + 1), group(final), False, part, parts)
-        send_pair(3, part)
     norm_group(final)
     got_norms[fs] = own_norms[...]
     norm_copies = [launch(own_norms, got_norms.at[fs], to_fs(index)) for index in fs_others]
     for part in range(parts):
         send_line(3, part)
-    settle(2)
-    settle(3, range(parts))
+    settle(0)
+    settle(1)
     for copies in (down_copies, square_copies, norm_copies):
         for copy in copies:
             copy.wait_recv()
@@ -510,11 +523,7 @@
     squares[...] = gathered(got_squares, fs_count)
     norms[...] = gathered(got_norms, fs_count)
     last_copies[1].wait_recv()
-    for j in range(2):
-        copy_of(
-            settled.at[0], out.at[:, cols(other * 2 + j)], to(far),
-            send_at=a2a[0], receive_at=a2a[j],
-        ).wait_recv()
+    settle_straight()
     for copy in pending:
         copy.wait_send()
 
@@ -574,8 +583,9 @@
             pltpu.VMEM((2, length, width), F32), wide, wide,
             wide, block, block, block, block, block, block,
             pltpu.VMEM((positions, depth), F32),
-            slots, slots, pltpu.VMEM((4, shard, depth), F32), pieces, pieces,
-            pltpu.VMEM((4, shard, depth), BF16),
+            slots, slots, pltpu.VMEM((2, shard, depth), F32), pieces,
+            pltpu.VMEM((2, line, shard, depth), BF16), pltpu.VMEM((shard, depth), BF16),
+            pltpu.VMEM((2, line, shard, depth), BF16),
             pltpu.VMEM((2, stat_rows, width), F32), half_sums, half_sums, half_sums,
             pltpu.VMEM((2, depth), F32), pltpu.VMEM((fs_count, 2, depth), F32),
             pltpu.VMEM((1, width), F32), pltpu.VMEM((tp_count, 1, width), F32),

time: 87.8 us -> 77.7 us (0.88)
  the two profiles are of different devices: /device:TPU:0 before, /device:TPU:1 now
where the time goes in v3:
time: 77.7 us; the launch traced here: 77.6 us
  Pallas kernels  76.9 us (99%)
    pallas_call x1, Pallas kernels, gradients(): pl.pallas_call(gradient_kernel, out_shape=(jax.ShapeDtypeStruct((position...  69 us
    pallas_call x1, Pallas kernels, weight_gradients(): pl.pallas_call(weight_kernel, out_shape=tuple((jax.ShapeDtypeStruct(grad_...  7.94 us

profile of v3, /device:TPU:1, one launch (start us, length us, event | category | flops | bytes accessed | tf_op | source)
XLA Modules:
  0.0 77.6 jit_solution(13841190900564491044)
XLA Ops:
  0.6 0.0 copy-start
  0.7 69.0 %shard_map.202 = (bf16[512,1024]{1,0:T(8,128)(2,1)S(1)}, bf16[2,512,1536]{2,1,0:T(8,128)(2,1)S(1)}, bf16[512,1536]{1,0:T(8,128)(2,1)S(1)}, f32[2,4,1536]{2,1,0:T...) custom-call(bf16[512,1024]{1,0:T(8,128)(2,1)} %hidden.1, ...), custom_call_target="tpu_custom_call" | custom-call | tf_op jit(solution)/shard_map/pallas_call | solution.py:559
  69.6 0.0 copy-done
  69.6 7.9 %shard_map.203 = (f32[1024,1536]{1,0:T(8,128)}, f32[1024,1536]{1,0:T(8,128)}, f32[1536,1024]{1,0:T(8,128)}, bf16[16,4096]{1,0:T(8,128)(2,1)}, f32[3,1536]{1,0:T(...) custom-call(bf16[512,1024]{1,0:T(8,128)(2,1)S(1)} %copy-done, ...), custom_call_target="tpu_custom_call" | custom-call | tf_op jit(solution)/shard_map/pallas_call | solution.py:684
Async XLA Ops:
  0.6 69.0 %copy-start = (bf16[512,1024]{1,0:T(8,128)(2,1)S(1)}, bf16[512,1024]{1,0:T(8,128)(2,1)}, u32[]{:S(2)}) copy-start(bf16[512,1024]{1,0:T(8,128)(2,1)} %hidden.1) | copy-start | bytes 3145732

commit v4 on v3

--- a/solution.py
+++ b/solution.py
@@ -17,6 +17,7 @@
 COPIES = 144
 ROWS = 512
 SLOTS = 3
+PARTS = 2
 ROOT_TWO_OVER_PI = 0.7978845608028654
 CUBIC = 0.044715
 
@@ -28,8 +29,8 @@
 def gradient_kernel(
     hidden_hbm, up_a_hbm, up_v_hbm, cot_hbm, w_a_hbm, w_v_hbm, down_hbm,
     taps_a_hbm, taps_v_hbm, bias_a_hbm, bias_v_hbm,
-    columns, all_g, all_m, sums, out, norms, down_norms, squares,
-    hidden, up, cot, weights, down, taps_a, taps_v, bias_a, bias_v, params,
+    grad_down, all_g, sums, out, norms, down_norms, squares,
+    columns, all_m, hidden, up, cot, weights, down, taps_a, taps_v, bias_a, bias_v, params,
     before, after, grads, gated, factor,
     own, to_sib, from_sib, to_sib_far, from_sib_far, to_far, from_far,
     terms, to_pair, from_pair, kept, to_line, from_line, settled, arrived,
@@ -271,18 +272,19 @@
 
     for g in range(group_count):
         relay_mixed(g)
+
+    def down_step(lanes):
+        value = contract_first(all_m[:, lanes], columns[...])
+        grad_down[lanes, :] = value
+        square = value * value
+        folded = square[:, :128]
+        for at in range(128, depth, 128):
+            folded = folded + square[:, at : at + 128]
+        own_down[:, lanes] = jnp.sum(folded.T, axis=0, keepdims=True)
+
     for copy in mixed_sib + mixed_relays:
         copy.wait_recv()
-    own_down[...] = jnp.zeros(own_down.shape, F32)
-
-    def down_step(lanes):
-        value = contract_first(columns[:, lanes], all_m[...])
-        own_down[...] += jnp.sum(value * value, axis=0, keepdims=True)
-
-    depth_chunks(down_step)
-    got_down[me] = own_down[...]
-    tp_others = [lax.rem(me + by, count) for by in range(1, count)]
-    down_copies = [launch(own_down, got_down.at[me], to(index)) for index in tp_others]
+    chunks(0, down_step)
 
     def combine(lanes):
         total = own[:, lanes] + from_sib[:, lanes].astype(F32) + from_far[:, lanes].astype(F32)
@@ -309,8 +311,8 @@
     final = group_count - 1
     backs, sent_g = [], {}
 
-    def cross(g, j):
-        here = all_g.at[core, rows(chip * 2 + j), group(g)]
+    def cross(g, j, block):
+        here = all_g.at[core, rows(block), group(g)]
         sent_g[g, j] = launch(here, here, to(far))
 
     near.wait_recv()
@@ -340,11 +342,13 @@
             beside.append(launch(here, here, to(sib)))
         for copy in beside:
             copy.wait_recv()
-        cross(g, 0)
         if g < final - 1:
-            cross(g, 1)
-    cross(final - 1, 1)
-    cross(final, 1)
+            cross(g, 0, me)
+            cross(g, 1, sib)
+        else:
+            cross(g, 0, chip * 2)
+    cross(final - 1, 1, chip * 2 + 1)
+    cross(final, 1, chip * 2 + 1)
     side_sums = launch(own_sums.at[1 - core], sib_sums, to(sib))
 
     loads[9].wait()
@@ -361,7 +365,7 @@
         return pl.ds(pl.multiple_of(blocks[k] * length + index * shard, shard), shard)
 
     pair_copies, line_copies, last_copies = {}, {}, {}
-    parts = 2 if depth % (2 * CHUNK) == 0 else 1
+    parts = PARTS if depth % (PARTS * CHUNK) == 0 else 1
     whole = pl.ds(0, depth)
 
     def part_of(part):
@@ -429,7 +433,8 @@
         started = []
         for g, j in which:
             sent_g[g, j].wait_recv()
-            there = all_g.at[core, rows(other * 2 + j), group(g)]
+            block = (far, diag)[j] if g < final - 1 else other * 2 + j
+            there = all_g.at[core, rows(block), group(g)]
             started.append(launch(there, there, to(sib)))
         return started
 
@@ -463,6 +468,11 @@
     send_pair(0)
     send_pair(1)
     started += relay((0, 1))
+    for g in range(1, group_count):
+        chunks(g, down_step)
+    got_down[me] = own_down[...]
+    tp_others = [lax.rem(me + by, count) for by in range(1, count)]
+    down_copies = [launch(own_down, got_down.at[me], to(index)) for index in tp_others]
     side_sums.wait_recv()
     chip_sums[...] = own_sums[core] + sib_sums[...]
     cross_sums = launch(chip_sums, far_sums, to(far))
@@ -503,12 +513,12 @@
         send_pair(3, part)
     send_line(2)
     norm_group(final)
+    settle(0)
+    settle(1)
+    for part in range(parts):
+        send_line(3, part)
     got_norms[fs] = own_norms[...]
     norm_copies = [launch(own_norms, got_norms.at[fs], to_fs(index)) for index in fs_others]
-    for part in range(parts):
-        send_line(3, part)
-    settle(0)
-    settle(1)
     for copies in (down_copies, square_copies, norm_copies):
         for copy in copies:
             copy.wait_recv()
@@ -559,9 +569,8 @@
     return pl.pallas_call(
         gradient_kernel,
         out_shape=(
-            jax.ShapeDtypeStruct((positions, depth), BF16),
+            jax.ShapeDtypeStruct((width, depth), F32),
             jax.ShapeDtypeStruct((2, positions, width), BF16),
-            jax.ShapeDtypeStruct((positions, width), BF16),
             jax.ShapeDtypeStruct((2, stat_rows, width), F32),
             jax.ShapeDtypeStruct((shard, depth * tp_count), BF16),
             jax.ShapeDtypeStruct((2, depth), F32),
@@ -569,8 +578,9 @@
             jax.ShapeDtypeStruct((2, stat_rows, 128), F32),
         ),
         in_specs=[hbm] * 11,
-        out_specs=(vmem,) * 8,
+        out_specs=(vmem,) * 7,
         scratch_shapes=[
+            pltpu.VMEM((positions, depth), BF16), pltpu.VMEM((positions, width), BF16),
             pltpu.VMEM(hidden_in.shape, BF16),
             pltpu.VMEM((2, length, width), BF16),
             pltpu.VMEM(cotangent.shape, BF16),
@@ -623,14 +633,16 @@
 
 
 def weight_kernel(
-    hidden, all_g, all_m, columns, sums, grad_in, norms, down_norms, squares,
+    hidden, all_g, grad_down, sums, grad_in, norms, down_norms, squares,
     w_act, w_val, w_down, input_out, conv_a, conv_v, bias_a, bias_v,
     rows_a, rows_v, rows_d, conv_rows,
     blocks, held_conv, held_rows, held_a, held_v, held_d, held_rows_a, held_rows_v,
     done, small_done,
 ):
     taps = conv_a.shape[0]
-    depth, width = hidden.shape[1], all_m.shape[1]
+    depth = hidden.shape[1]
+    down_copy = pltpu.make_async_copy(grad_down, w_down, small_done.at[9])
+    down_copy.start()
     for r in range(2):
         held_conv[r] = sums[r, :taps, :]
     held_a[...] = sums[0, taps, :]
@@ -657,7 +669,6 @@
         copy.start()
     jobs = [(hidden, all_g.at[0], w_act, at) for at in range(0, depth, ROWS)]
     jobs += [(hidden, all_g.at[1], w_val, at) for at in range(0, depth, ROWS)]
-    jobs += [(all_m, columns, w_down, at) for at in range(0, width, ROWS)]
     stored = []
     for number, (left, right, target, at) in enumerate(jobs):
         slot = number % SLOTS
@@ -669,14 +680,14 @@
             blocks.at[slot, :, pl.ds(0, size)], target.at[pl.ds(at, ROWS), :], done.at[slot]
         ))
         stored[number].start()
-    for copy in stored[-SLOTS:] + flying:
+    for copy in stored[-SLOTS:] + flying + [down_copy]:
         copy.wait()
 
 
-def weight_gradients(hidden_in, all_g, all_m, columns, sums, grad_in, norms, down_norms, squares):
-    depth, width = hidden_in.shape[1], all_m.shape[1]
+def weight_gradients(hidden_in, all_g, grad_down, sums, grad_in, norms, down_norms, squares):
+    width, depth = grad_down.shape
     taps = sums.shape[1] - 1
-    operands = (hidden_in, all_g, all_m, columns, sums, grad_in, norms, down_norms, squares)
+    operands = (hidden_in, all_g, grad_down, sums, grad_in, norms, down_norms, squares)
     shapes = (
         (depth, width), (depth, width), (width, depth), None, (taps, width), (taps, width),
         (width,), (width,), (depth,), (depth,), (width,), (2, taps),
@@ -691,11 +702,11 @@
         in_specs=[pl.BlockSpec(memory_space=pltpu.VMEM)] * len(operands),
         out_specs=(pl.BlockSpec(memory_space=pltpu.HBM),) * len(shapes),
         scratch_shapes=[
-            pltpu.VMEM((SLOTS, ROWS, max(depth, width)), F32),
+            pltpu.VMEM((SLOTS, ROWS, width), F32),
             pltpu.VMEM((2, taps, width), F32), pltpu.VMEM((2, taps), F32),
             pltpu.VMEM((width,), F32), pltpu.VMEM((width,), F32), pltpu.VMEM((width,), F32),
             pltpu.VMEM((depth,), F32), pltpu.VMEM((depth,), F32),
-            pltpu.SemaphoreType.DMA((SLOTS,)), pltpu.SemaphoreType.DMA((9,)),
+            pltpu.SemaphoreType.DMA((SLOTS,)), pltpu.SemaphoreType.DMA((10,)),
         ],
         compiler_params=pltpu.CompilerParams(vmem_limit_bytes=24 * 1024 * 1024),
     )(*operands)
@@ -705,7 +716,7 @@
     hidden_in, up_act, up_val, cotangent, w_act, w_val, w_down,
     conv_act, conv_val, bias_act, bias_val,
 ):
-    columns, all_g, all_m, sums, grad_in, norms, down_norms, squares = gradients(
+    grad_down, all_g, sums, grad_in, norms, down_norms, squares = gradients(
         hidden_in, up_act, up_val, cotangent, w_act, w_val, w_down,
         conv_act, conv_val, bias_act, bias_val,
     )
@@ -713,7 +724,7 @@
         grad_w_act, grad_w_val, grad_w_down, grad_input, conv_a, conv_v, bias_a, bias_v,
         rows_a, rows_v, rows_d, conv_rows,
     ) = weight_gradients(
-        hidden_in, all_g, all_m, columns, sums, grad_in, norms, down_norms, squares
+        hidden_in, all_g, grad_down, sums, grad_in, norms, down_norms, squares
     )
     return (
         grad_input, grad_w_act, grad_w_val, grad_w_down, conv_a, conv_v,

time: 77.7 us -> 77.2 us (level)
  the two profiles are of different devices: /device:TPU:1 before, /device:TPU:0 now
where the time goes in v4:
time: 77.2 us; the launch traced here: 77 us
  Pallas kernels  76.4 us (99%)
    pallas_call x1, Pallas kernels, gradients(): pl.pallas_call(gradient_kernel, out_shape=(jax.ShapeDtypeStruct((width, d...  69.6 us
    pallas_call x1, Pallas kernels, weight_gradients(): pl.pallas_call(weight_kernel, out_shape=tuple((jax.ShapeDtypeStruct(grad_...  6.79 us

profile of v4, /device:TPU:0, one launch (start us, length us, event | category | flops | bytes accessed | tf_op | source)
XLA Modules:
  0.0 77.0 jit_solution(2398598063836217977)
XLA Ops:
  0.6 0.0 copy-start
  0.7 69.6 %shard_map.202 = (f32[1536,1024]{1,0:T(8,128)S(1)}, bf16[2,512,1536]{2,1,0:T(8,128)(2,1)S(1)}, f32[2,4,1536]{2,1,0:T(4,128)S(1)}, bf16[16,4096]{1,0:T(8,128)(2,1...) custom-call(bf16[512,1024]{1,0:T(8,128)(2,1)} %hidden.1, ...), custom_call_target="tpu_custom_call" | custom-call | tf_op jit(solution)/shard_map/pallas_call | solution.py:569
  70.2 0.0 copy-done
  70.2 6.8 %shard_map.203 = (f32[1024,1536]{1,0:T(8,128)}, f32[1024,1536]{1,0:T(8,128)}, f32[1536,1024]{1,0:T(8,128)}, bf16[16,4096]{1,0:T(8,128)(2,1)}, f32[3,1536]{1,0:T(...) custom-call(bf16[512,1024]{1,0:T(8,128)(2,1)S(1)} %copy-done, ...), custom_call_target="tpu_custom_call" | custom-call | tf_op jit(solution)/shard_map/pallas_call | solution.py:695
Async XLA Ops:
  0.6 69.6 %copy-start = (bf16[512,1024]{1,0:T(8,128)(2,1)S(1)}, bf16[512,1024]{1,0:T(8,128)(2,1)}, u32[]{:S(2)}) copy-start(bf16[512,1024]{1,0:T(8,128)(2,1)} %hidden.1) | copy-start | bytes 3145732
